TPU v7x, 256 devices: a whole 4x4x8 slice. The times are simulated.
256 devices in a mesh: sp: 64 (over z, x, core), tp: 4 (over y).
Axes of the slice: x: 4, y: 4, z: 8, core: 2. Of those that a mesh axis runs over, the one named last changes fastest.
Arguments:
- residual: bfloat16 [16384, 2048], P('sp', 'tp'), may hold values from -8 to 8
- query_latent: bfloat16 [16384, 512], P('sp'), may hold values from -6 to 6
- shared_latent: bfloat16 [16384, 256], P('sp'), may hold values from -6 to 6
- rotary_key: bfloat16 [16384, 32], P('sp'), may hold values from -300 to 300
- query_gain: float32 [512], replicated, may hold values from 0.1 to 1.9
- latent_gain: float32 [256], replicated, may hold values from 0.1 to 1.9
- query_narrow: bfloat16 [512, 384], P(None, 'tp'), may hold values from -0.5 to 0.5
- key_narrow: bfloat16 [256, 256], P(None, 'tp'), may hold values from -0.375 to 0.375
- value_narrow: bfloat16 [256, 256], P(None, 'tp'), may hold values from -0.375 to 0.375
- query_wide: bfloat16 [512, 640], P(None, 'tp'), may hold values from -0.5 to 0.5
- key_wide: bfloat16 [256, 512], P(None, 'tp'), may hold values from -0.375 to 0.375
- value_wide: bfloat16 [256, 512], P(None, 'tp'), may hold values from -0.375 to 0.375
- output_narrow: bfloat16 [256, 2048], P('tp'), may hold values from -1.75 to 1.75
- output_wide: bfloat16 [512, 2048], P('tp'), may hold values from -1.75 to 1.75
- first_gain: float32 [2048], P('tp'), may hold values from 0.1 to 1.9
- first_bias: float32 [2048], P('tp'), may hold values from -1.5 to 1.5
- gate_weight: bfloat16 [2048, 5632], P('sp', 'tp'), may hold values from -0.125 to 0.125
- up_weight: bfloat16 [2048, 5632], P('sp', 'tp'), may hold values from -0.125 to 0.125
- down_weight: bfloat16 [5632, 2048], P('tp', 'sp'), may hold values from -0.078125 to 0.078125
- second_gain: float32 [2048], P('tp'), may hold values from 0.1 to 1.9
- second_bias: float32 [2048], P('tp'), may hold values from -1.5 to 1.5
Outputs:
- layer_out: bfloat16 [16384, 2048], P('sp', 'tp')
All inputs are finite; a program needn't handle non-finite values.
Results may differ from a plain program's by a relative error of at most 0.017.
The roundings to bfloat16 on the way count: a program that leaves them out, or rounds other values in their place, can miss the bound.
Values may be sent and summed in bfloat16 or wider, within the bound.
A program may use at most 192 MiB of HBM per device.

v0:
```python
import jax
import jax.numpy as jnp
from jax import lax
from jax.sharding import PartitionSpec as P

ROPE = 32
NOPE_A = 64
V_A = 64
NOPE_B = 128
V_B = 128
GRID_W = 64


EPS_ROOT = 1e-06
EPS_LAYER = 1e-05
THETA = 10000.0
DEEP_ALPHA = 2.0**0.25


def in_one_piece(arrays, axis, dim, along):
    ends, at = ([], 0)
    for a in arrays[:-1]:
        at += a.shape[along]
        ends.append(at)
    both = jnp.concatenate(arrays, axis=along)
    return tuple(jnp.split(lax.all_gather(both, axis, axis=dim, tiled=True), ends, axis=along))


def split_up(x, dim, size):
    before, after = (x.shape[:dim], x.shape[dim + 1 :])
    return jnp.moveaxis(x.reshape(*before, size, -1, *after), dim, 0)


def sum_at_owner(x, axis, dim):
    size = lax.axis_size(axis)
    pieces = lax.all_to_all(split_up(x, dim, size), axis, 0, 0, tiled=True)
    return jnp.sum(pieces.astype(jnp.float32), axis=0)


def sent_to_all(x, axis):
    copies = jnp.broadcast_to(x, (lax.axis_size(axis), *x.shape))
    return lax.all_to_all(copies, axis, split_axis=0, concat_axis=0, tiled=True)


def of_everyone(x, axis):
    return sent_to_all(x, axis).sum(axis=0)


def in_one(arrays, axis):
    ends = [0]
    for a in arrays:
        ends.append(ends[-1] + a.size)
    so_far = of_everyone(jnp.concatenate([a.ravel() for a in arrays]), axis)
    return tuple((so_far[b:e].reshape(a.shape) for a, b, e in zip(arrays, ends, ends[1:])))


def in_order(pieces, dim):
    shape = list(pieces.shape[1:])
    shape[dim] *= pieces.shape[0]
    return jnp.moveaxis(pieces, 0, dim).reshape(shape)


def collect(x, axis, dim):
    return in_order(sent_to_all(x, axis), dim)


def rotate(half_part, angle):
    lower, upper = jnp.split(half_part, 2, axis=-1)
    cosine = jnp.cos(angle)
    sine = jnp.sin(angle)
    return jnp.concatenate([lower * cosine - upper * sine, upper * cosine + lower * sine], axis=-1)


def turn_axial(values_in, positions):
    quarter = values_in.shape[-1] // 4
    freqs = THETA ** (-(2.0 * jnp.arange(quarter, dtype=jnp.float32)) / (2 * quarter))
    row_angle = (positions // GRID_W).astype(jnp.float32)[:, None, None] * freqs
    col_angle = (positions % GRID_W).astype(jnp.float32)[:, None, None] * freqs
    first_half, second_half = jnp.split(values_in, 2, axis=-1)
    return jnp.concatenate([rotate(first_half, row_angle), rotate(second_half, col_angle)], axis=-1)


def root_scale(latent, gain):
    floated = latent.astype(jnp.float32)
    return (
        floated * lax.rsqrt(jnp.mean(floated * floated, axis=-1, keepdims=True) + EPS_ROOT) * gain
    )


def make_query(normed, weight, plain_dim, positions):
    product = jnp.dot(normed, weight, preferred_element_type=jnp.float32)
    head_count = weight.shape[1] // (plain_dim + ROPE)
    product = product.reshape(product.shape[0], head_count, plain_dim + ROPE)
    turned = turn_axial(product[:, :, plain_dim:], positions)
    return jnp.concatenate([product[:, :, :plain_dim], turned], axis=-1).astype(jnp.bfloat16)


def fresh_state(row_count, head_count, value_dim):
    largest = jnp.full((head_count, row_count), -jnp.inf, jnp.float32)
    totals = jnp.zeros((head_count, row_count), jnp.float32)
    weighted = jnp.zeros((row_count, head_count, value_dim), jnp.float32)
    return (largest, totals, weighted)


def update(state_now, queries, key_rows, value_rows, rotary_rows, plain_dim):
    largest, totals, weighted = state_now
    score_scale = queries.shape[2] ** (-0.5)
    scores = jnp.einsum(
        "qhd,khd->hqk", queries[:, :, :plain_dim], key_rows, preferred_element_type=jnp.float32
    )
    scores = scores + jnp.einsum(
        "qhd,kd->hqk", queries[:, :, plain_dim:], rotary_rows, preferred_element_type=jnp.float32
    )
    scores = scores * score_scale
    new_largest = jnp.max(scores, axis=-1)
    factor = jnp.exp(largest - new_largest)
    raised = jnp.exp(scores - new_largest[:, :, None])
    totals = totals * factor + jnp.sum(raised, axis=-1)
    added = jnp.einsum(
        "hqk,khd->qhd", raised.astype(jnp.bfloat16), value_rows, preferred_element_type=jnp.float32
    )
    weighted = weighted * factor.T[:, :, None] + added
    return (new_largest, totals, weighted)


def finish(state_now):
    largest, totals, weighted = state_now
    output = (weighted / totals.T[:, :, None]).astype(jnp.bfloat16)
    return output.reshape(output.shape[0], output.shape[1] * output.shape[2])


def finish_norm(summed, sums, squares, gain, bias, width_total):
    center = sums / width_total
    spread = squares / width_total - center * center
    normed = (summed - center[:, None]) * lax.rsqrt(spread + EPS_LAYER)[:, None]
    return (normed * gain + bias).astype(jnp.bfloat16)


def body(
    residual,
    query_latent,
    shared_latent,
    rotary_key,
    query_gain,
    latent_gain,
    query_narrow,
    key_narrow,
    value_narrow,
    query_wide,
    key_wide,
    value_wide,
    output_narrow,
    output_wide,
    first_gain,
    first_bias,
    gate_weight,
    up_weight,
    down_weight,
    second_gain,
    second_bias,
):
    row_count = residual.shape[0]
    offset = lax.axis_index("sp") * row_count
    positions = offset + jnp.arange(row_count, dtype=jnp.int32)
    query_normed = root_scale(query_latent, query_gain).astype(jnp.bfloat16)
    narrow_queries = make_query(query_normed, query_narrow, NOPE_A, positions)
    wide_queries = make_query(query_normed, query_wide, NOPE_B, positions)
    narrow_heads = narrow_queries.shape[1]
    wide_heads = wide_queries.shape[1]
    start_state = (
        fresh_state(row_count, narrow_heads, V_A),
        fresh_state(row_count, wide_heads, V_B),
    )
    shard_rows = in_one_piece((shared_latent, rotary_key), "sp", 0, 1)
    latent_rows = shard_rows[0]
    normed = root_scale(latent_rows, latent_gain).astype(jnp.bfloat16)
    count = latent_rows.shape[0]
    narrow_keys = jnp.dot(normed, key_narrow, preferred_element_type=jnp.float32).astype(
        jnp.bfloat16
    )
    narrow_vals = jnp.dot(normed, value_narrow, preferred_element_type=jnp.float32).astype(
        jnp.bfloat16
    )
    wide_keys = jnp.dot(normed, key_wide, preferred_element_type=jnp.float32).astype(jnp.bfloat16)
    wide_vals = jnp.dot(normed, value_wide, preferred_element_type=jnp.float32).astype(jnp.bfloat16)
    key_positions = jnp.arange(count, dtype=jnp.int32)
    rotated = turn_axial(shard_rows[1].astype(jnp.float32)[:, None, :], key_positions)[
        :, 0, :
    ].astype(jnp.bfloat16)
    count = rotated.shape[0]
    narrow_state = update(
        start_state[0],
        narrow_queries,
        narrow_keys.reshape(count, narrow_heads, NOPE_A),
        narrow_vals.reshape(count, narrow_heads, V_A),
        rotated,
        NOPE_A,
    )
    wide_state = update(
        start_state[1],
        wide_queries,
        wide_keys.reshape(count, wide_heads, NOPE_B),
        wide_vals.reshape(count, wide_heads, V_B),
        rotated,
        NOPE_B,
    )
    narrow_out = finish(narrow_state)
    wide_out = finish(wide_state)
    terms = jnp.dot(narrow_out, output_narrow, preferred_element_type=jnp.float32)
    terms = terms + jnp.dot(wide_out, output_wide, preferred_element_type=jnp.float32)
    mixed = sum_at_owner(terms.astype(jnp.bfloat16), "tp", 1)
    width_total = mixed.shape[1] * lax.axis_size("tp")
    summed = DEEP_ALPHA * residual.astype(jnp.float32) + mixed
    sums, squares = in_one((jnp.sum(summed, axis=1), jnp.sum(summed * summed, axis=1)), "tp")
    normed_first = finish_norm(summed, sums, squares, first_gain, first_bias, width_total)
    full_rows = collect(normed_first, "tp", 1)
    shard_rows = in_one_piece((gate_weight, up_weight), "sp", 0, 1)
    gate_part = jnp.dot(full_rows, shard_rows[0], preferred_element_type=jnp.float32)
    lifted_part = jnp.dot(full_rows, shard_rows[1], preferred_element_type=jnp.float32)
    hidden = (jax.nn.silu(gate_part) * lifted_part).astype(jnp.bfloat16)
    feed_terms = jnp.dot(
        hidden,
        lax.all_gather(down_weight, "sp", axis=1, tiled=True),
        preferred_element_type=jnp.float32,
    )
    feed = sum_at_owner(feed_terms.astype(jnp.bfloat16), "tp", 1)
    summed_two = DEEP_ALPHA * normed_first.astype(jnp.float32) + feed
    sums_two, squares_two = in_one(
        (jnp.sum(summed_two, axis=1), jnp.sum(summed_two * summed_two, axis=1)), "tp"
    )
    return finish_norm(summed_two, sums_two, squares_two, second_gain, second_bias, width_total)


def solution(mesh):
    return jax.shard_map(
        body,
        mesh=mesh,
        in_specs=(
            P("sp", "tp"),
            P("sp", None),
            P("sp", None),
            P("sp", None),
            P(),
            P(),
            P(None, "tp"),
            P(None, "tp"),
            P(None, "tp"),
            P(None, "tp"),
            P(None, "tp"),
            P(None, "tp"),
            P("tp", None),
            P("tp", None),
            P("tp"),
            P("tp"),
            P("sp", "tp"),
            P("sp", "tp"),
            P("tp", "sp"),
            P("tp"),
            P("tp"),
        ),
        out_specs=P("sp", "tp"),
        check_vma=False,
    )
```

profile of v0, /device:TPU:1, one launch (start us, length us, event | category | flops | bytes accessed | tf_op | source)
XLA Modules:
  0.0 313.4 jit_solution(8049191181758371652)
XLA Ops:
  6.5 1.1 copy.41
  7.6 1.4 pad_maximum_fusion.4
  9.0 0.0 all-gather.4.cloned.1.call-update
  9.0 0.0 all-gather.6.cloned.1.call-start
  9.1 1.6 pad_maximum_fusion.1
  10.7 0.0 all-gather.6.cloned.1.call-update
  10.7 0.0 all-gather.8.cloned.1.call-start
  10.8 0.7 all-gather.8.cloned.1.call-update
  11.5 1.1 fusion.72
  12.6 1.3 convolution_bitcast_fusion.4
  13.9 1.3 convolution_bitcast_fusion.5
  15.2 0.2 fusion.133
  15.4 85.9 %all-gather.4.cloned.1.call-done = bf16[16384,288]{0,1:T(8,128)(2,1)} async-done(((bf16[256,288]{0,1:T(8,128)(2,1)}), bf16[16384,288]{0,1:T(8,128)(2,1)}) %all-gather.4.cloned.1.call-update) | async-done | bytes 9437200 | tf_op jit(solution)/shard_map/all_gather | solution.py:26
  101.3 5.1 %fusion.4 = f32[16384]{0:T(1024)S(1)} fusion(bf16[16384,288]{0,1:T(8,128)(2,1)} %all-gather.4.cloned.1.call-done), kind=kLoop, calls=%fused_computation.14 | loop fusion | flops 12566528 | bytes 8454144 | tf_op jit(solution)/shard_map/reduce_sum | solution.py:86
  106.4 1.4 fusion.62
  107.8 4.4 %fusion.84 = (bf16[16384,8]{0,1:T(8,128)(2,1)S(1)}, bf16[16384,8]{0,1:T(8,128)(2,1)S(1)}, bf16[16384,8]{0,1:T(8,128)(2,1)S(1)}, bf16[16384,8]{0,1:T(8,128)(2,1)S(1)}) fusion(f32[16384,1,32]{0,2,1:T(8,128)S(1)} %fusion.62, f32[8]{0:T(128)S(1)} %multiply_power_fusion, f32[16384]{0:T(1024)S(1)} %get-tuple-element.43, f32[16384]{0:T(1024)S(1)} %get-tuple-element.44), kind=kLoop, calls=%fused_computation.90 | loop fusion | flops 2359296 | bytes 3276832 | tf_op jit(solution)/shard_map/concatenate | solution.py:80
  112.2 0.0 copy-start.4
  112.2 0.0 copy-start.5
  112.2 8.1 %convolution_bitcast_fusion.2 = f32[1,256,16384]{2,1,0:T(8,128)} fusion(bf16[16384,8]{0,1:T(8,128)(2,1)S(1)} %get-tuple-element.13, bf16[16384,8]{0,1:T(8,128)(2,1)S(1)} %get-tuple-element.14, bf16[16384,8]{0,1:T(8,128)(2,1)S(1)} %get-tuple-element.10, bf16[16384,8]{0,1:T(8,128)(2,1)S(1)} %get-tuple-element.9, bf16[256,1,8]{0,2,1:T(8,128)(2,1)S(1)} %get-tuple-element.25, ...), kind=kOutput, calls=%fused_computation.2 | convolution fusion | flops 272695296 | bytes 17842176 | tf_op jit(solution)/shard_map/qhd,kd->hqk/dot_general | solution.py:111
  120.3 14.5 %fusion.167 = (f32[256]{0:T(256)S(1)}, f32[1,256,16384]{2,1,0:T(8,128)}) fusion(f32[1,256,16384]{2,1,0:T(8,128)} %convolution_bitcast_fusion.2, bf16[256,64]{0,1:T(8,128)(2,1)S(1)} %copy-done.4, f32[256]{0:T(256)S(1)} %copy-done.5, f32[16384]{0:T(1024)S(1)} %add_rsqrt_fusion, bf16[16384,288]{0,1:T(8,128)(2,1)} %all-gather.4.cloned.1.call-done, ...), kind=kOutput, calls=%fused_computation.191 | convolution fusion | flops 1104150272 | bytes 42076160 | tf_op jit(solution)/shard_map/qhd,khd->hqk/dot_general | solution.py:108
  134.8 8.1 %convolution_bitcast_fusion = f32[1,256,16384]{2,1,0:T(8,128)} fusion(bf16[16384,8]{0,1:T(8,128)(2,1)S(1)} %get-tuple-element.13, bf16[16384,8]{0,1:T(8,128)(2,1)S(1)} %get-tuple-element.14, bf16[16384,8]{0,1:T(8,128)(2,1)S(1)} %get-tuple-element.10, bf16[16384,8]{0,1:T(8,128)(2,1)S(1)} %get-tuple-element.9, bf16[256,1,8]{0,2,1:T(8,128)(2,1)S(1)} %get-tuple-element.28, ...), kind=kOutput, calls=%fused_computation | convolution fusion | flops 272695296 | bytes 17842176 | tf_op jit(solution)/shard_map/qhd,kd->hqk/dot_general | solution.py:111
  142.9 8.2 %fusion.7 = f32[256]{0:T(256)S(1)} fusion(f32[1,256,16384]{2,1,0:T(8,128)} %get-tuple-element.42, f32[256]{0:T(256)S(1)} %get-tuple-element.41), kind=kLoop, calls=%fused_computation.19 | loop fusion | flops 8388352 | bytes 16779264 | tf_op jit(solution)/shard_map/reduce_sum | solution.py:118
  151.1 15.2 %fusion.164 = (f32[256]{0:T(256)S(1)}, f32[1,256,16384]{2,1,0:T(8,128)}) fusion(f32[1,256,16384]{2,1,0:T(8,128)} %convolution_bitcast_fusion, bf16[256,128]{1,0:T(8,128)(2,1)S(1)} %copy-done.3, f32[256]{0:T(256)S(1)} %copy-done.5, f32[16384]{0:T(1024)S(1)} %add_rsqrt_fusion, bf16[16384,288]{0,1:T(8,128)(2,1)} %all-gather.4.cloned.1.call-done, ...), kind=kOutput, calls=%fused_computation.190 | convolution fusion | flops 2178940672 | bytes 42141696 | tf_op jit(solution)/shard_map/qhd,khd->hqk/dot_general | solution.py:108
  166.3 8.7 %fusion.9 = f32[256]{0:T(256)S(1)} fusion(f32[1,256,16384]{2,1,0:T(8,128)} %get-tuple-element.40, f32[256]{0:T(256)S(1)} %get-tuple-element.39), kind=kLoop, calls=%fused_computation.21 | loop fusion | flops 8388352 | bytes 16779264 | tf_op jit(solution)/shard_map/reduce_sum | solution.py:118
  175.1 0.0 copy-start.11
  175.1 11.8 %fusion.44 = bf16[256,128]{0,1:T(8,128)(2,1)S(1)} fusion(f32[1,256,16384]{2,1,0:T(8,128)} %get-tuple-element.40, f32[256]{0:T(256)S(1)} %get-tuple-element.39, bf16[256,128]{1,0:T(8,128)(2,1)S(1)} %copy-done.10, f32[256]{0:T(256)S(1)} %get-tuple-element.38, f32[256]{0:T(256)S(1)} %get-tuple-element.37, f32[256]{0:T(256)S(1)} %copy-done.5, ...), kind=kOutput, calls=%fused_computation.46 | convolution fusion | flops 2174844928 | bytes 25366528 | tf_op jit(solution)/shard_map/hqk,khd->qhd/dot_general | solution.py:119
  186.9 0.5 fusion.170
  187.4 0.0 copy-start.2
  187.4 11.1 %fusion.59 = bf16[256,64]{0,1:T(8,128)(2,1)S(1)} fusion(f32[1,256,16384]{2,1,0:T(8,128)} %get-tuple-element.42, f32[256]{0:T(256)S(1)} %get-tuple-element.41, bf16[256,64]{0,1:T(8,128)(2,1)S(1)} %copy-done.11, f32[256]{0:T(256)S(1)} %get-tuple-element.36, f32[256]{0:T(256)S(1)} %get-tuple-element.35, f32[256]{0:T(256)S(1)} %copy-done.5, ...), kind=kOutput, calls=%fused_computation.51 | convolution fusion | flops 1100005376 | bytes 25300992 | tf_op jit(solution)/shard_map/hqk,khd->qhd/dot_general | solution.py:119
  198.5 0.5 fusion.26
  199.0 0.1 copy.62
  199.1 18.0 %all_to_all.27 = bf16[4,256,512]{2,1,0:T(8,128)(2,1)S(1)} all-to-all(bf16[4,256,512]{2,1,0:T(8,128)(2,1)S(1)} %bitcast.138), channel_id=1, replica_groups=mesh['sp'=64,'tp'=4] {'tp'}, dimensions={0} | all-to-all | bytes 2097152 | tf_op jit(solution)/shard_map/all_to_all | solution.py:36
  217.1 0.1 convert_reduce_fusion.1
  217.3 0.2 fusion.87
  217.5 6.6 %all_to_all.28 = f32[4,1,512]{2,1,0:T(1,128)S(1)} all-to-all(f32[4,1,512]{2,1,0:T(1,128)S(1)} %broadcast_in_dim.16), channel_id=1, replica_groups=mesh['sp'=64,'tp'=4] {'tp'}, dimensions={0} | all-to-all | bytes 16384 | tf_op jit(solution)/shard_map/all_to_all | solution.py:42
  224.2 0.2 add_convert_fusion.1
  224.3 0.1 copy.46
  224.5 0.1 broadcast_in_dim.17
  224.5 14.5 %all_to_all.29 = bf16[4,256,512]{1,2,0:T(8,128)(2,1)S(1)} all-to-all(bf16[4,256,512]{1,2,0:T(8,128)(2,1)S(1)} %broadcast_in_dim.17), channel_id=1, replica_groups=mesh['sp'=64,'tp'=4] {'tp'}, dimensions={0} | all-to-all | bytes 2097152 | tf_op jit(solution)/shard_map/all_to_all | solution.py:42
  239.0 5.8 %fusion.21 = f32[256,1408]{1,0:T(8,128)} fusion(bf16[256,2048]{0,1:T(8,128)(2,1)S(1)} %bitcast.140, bf16[2048,2816]{1,0:T(8,128)(2,1)} %all-gather.6.cloned.1.call-done), kind=kOutput, calls=%fused_computation.31 | convolution fusion | flops 1476395008 | bytes 8257536 | tf_op jit(solution)/shard_map/dot_general | solution.py:218
  244.8 27.4 %all-gather.8.cloned.1.call-done = bf16[1408,2048]{0,1:T(8,128)(2,1)} async-done(((bf16[1408,32]{0,1:T(8,128)(2,1)}), bf16[1408,2048]{0,1:T(8,128)(2,1)}) %all-gather.8.cloned.1.call-update) | async-done | bytes 5767184 | tf_op jit(solution)/shard_map/all_gather | solution.py:223
  272.2 8.3 %convolution_convert_fusion.4 = bf16[256,2048]{1,0:T(8,128)(2,1)S(1)} fusion(bf16[1408,2048]{0,1:T(8,128)(2,1)} %all-gather.8.cloned.1.call-done, bf16[256,2048]{0,1:T(8,128)(2,1)S(1)} %bitcast.141, bf16[2048,2816]{1,0:T(8,128)(2,1)} %all-gather.6.cloned.1.call-done, f32[256,1408]{1,0:T(8,128)} %fusion.21), kind=kOutput, calls=%fused_computation.37 | convolution fusion | flops 2955476992 | bytes 15073280 | tf_op jit(solution)/shard_map/dot_general | solution.py:221
  280.5 0.1 copy.61
  280.6 18.4 %all_to_all.30 = bf16[4,256,512]{2,1,0:T(8,128)(2,1)S(1)} all-to-all(bf16[4,256,512]{2,1,0:T(8,128)(2,1)S(1)} %bitcast.139), channel_id=1, replica_groups=mesh['sp'=64,'tp'=4] {'tp'}, dimensions={0} | all-to-all | bytes 2097152 | tf_op jit(solution)/shard_map/all_to_all | solution.py:36
  299.0 0.1 convert_reduce_fusion
  299.2 0.2 fusion.88
  299.4 6.5 %all_to_all.31 = f32[4,1,512]{2,1,0:T(1,128)S(1)} all-to-all(f32[4,1,512]{2,1,0:T(1,128)S(1)} %broadcast_in_dim.18), channel_id=1, replica_groups=mesh['sp'=64,'tp'=4] {'tp'}, dimensions={0} | all-to-all | bytes 16384 | tf_op jit(solution)/shard_map/all_to_all | solution.py:42
  306.0 0.9 add_convert_fusion
  (37 shorter events, 0.2 us)
Async XLA Ops:
  6.5 180.4 %copy-start = (bf16[128,2048]{1,0:T(8,128)(2,1)S(1)}, bf16[128,2048]{1,0:T(8,128)(2,1)}, u32[]{:S(2)}) copy-start(bf16[128,2048]{1,0:T(8,128)(2,1)} %param.34) | copy-start | bytes 1572868
  6.5 94.7 %all-gather.4.cloned.1.call-start = ((), (), s32[]{:S(2)}) async-start(), calls=%async_computation.5 | async-start | bytes 9584640 | tf_op jit(solution)/shard_map/all_gather | solution.py:26
  9.0 230.0 %all-gather.6.cloned.1.call-start = ((), (), s32[]{:S(2)}) async-start(), calls=%async_computation.6 | async-start | bytes 11714560 | tf_op jit(solution)/shard_map/all_gather | solution.py:26
  10.7 261.5 %all-gather.8.cloned.1.call-start = ((), (), s32[]{:S(2)}) async-start(), calls=%async_computation.7 | async-start | bytes 5857280 | tf_op jit(solution)/shard_map/all_gather | solution.py:223
  112.2 8.1 %copy-start.4 = (bf16[256,64]{0,1:T(8,128)(2,1)S(1)}, bf16[256,64]{0,1:T(8,128)(2,1)}, u32[]{:S(2)}) copy-start(bf16[256,64]{0,1:T(8,128)(2,1)} %param.28) | copy-start | bytes 98308
  112.2 8.1 %copy-start.5 = (f32[256]{0:T(256)S(1)}, f32[256]{0:T(256)}, u32[]{:S(2)}) copy-start(f32[256]{0:T(256)} %param.26) | copy-start | bytes 3076
  142.9 8.2 %copy-start.3 = (bf16[256,128]{1,0:T(8,128)(2,1)S(1)}, bf16[256,128]{1,0:T(8,128)(2,1)}, u32[]{:S(2)}) copy-start(bf16[256,128]{1,0:T(8,128)(2,1)} %param.31) | copy-start | bytes 196612
  166.3 8.7 %copy-start.10 = (bf16[256,128]{1,0:T(8,128)(2,1)S(1)}, bf16[256,128]{1,0:T(8,128)(2,1)}, u32[]{:S(2)}) copy-start(bf16[256,128]{1,0:T(8,128)(2,1)} %param.32) | copy-start | bytes 196612
  175.1 12.3 %copy-start.11 = (bf16[256,64]{0,1:T(8,128)(2,1)S(1)}, bf16[256,64]{0,1:T(8,128)(2,1)}, u32[]{:S(2)}) copy-start(bf16[256,64]{0,1:T(8,128)(2,1)} %param.29) | copy-start | bytes 98308
  187.4 11.1 %copy-start.2 = (bf16[64,2048]{1,0:T(8,128)(2,1)S(1)}, bf16[64,2048]{1,0:T(8,128)(2,1)}, u32[]{:S(2)}) copy-start(bf16[64,2048]{1,0:T(8,128)(2,1)} %param.33) | copy-start | bytes 786436
  187.4 29.9 %copy-start.1 = (bf16[256,512]{1,0:T(8,128)(2,1)S(1)}, bf16[256,512]{1,0:T(8,128)(2,1)}, u32[]{:S(2)}) copy-start(bf16[256,512]{1,0:T(8,128)(2,1)} %param.21) | copy-start | bytes 786436
  198.5 25.6 %copy-start.6 = (f32[512]{0:T(512)S(1)}, f32[512]{0:T(512)}, u32[]{:S(2)}) copy-start(f32[512]{0:T(512)} %param.36) | copy-start | bytes 6148
  198.5 25.6 %copy-start.7 = (f32[512]{0:T(512)S(1)}, f32[512]{0:T(512)}, u32[]{:S(2)}) copy-start(f32[512]{0:T(512)} %param.35) | copy-start | bytes 6148
  244.8 61.1 %copy-start.8 = (f32[512]{0:T(512)S(1)}, f32[512]{0:T(512)}, u32[]{:S(2)}) copy-start(f32[512]{0:T(512)} %param.41) | copy-start | bytes 6148
  244.8 61.2 %copy-start.9 = (f32[512]{0:T(512)S(1)}, f32[512]{0:T(512)}, u32[]{:S(2)}) copy-start(f32[512]{0:T(512)} %param.40) | copy-start | bytes 6148
Sparse Core Ops, SparseCore 0:
  10.0 91.2 all-gather.3
  104.0 88.4 all-gather.5
  195.3 76.8 all-gather.7
where the time goes:
time: 314 us; the launch traced here: 313 us
  waiting for transfers between devices  114 us (36%)
  matrix products  86.3 us (27%)
  blocking collectives  64.1 us (20%)
  other arithmetic  33.9 us (11%)
  between operations  13.4 us (4%)
    all_gather x2, waiting for transfers between devices, in_one_piece(): lax.all_gather(both, axis, axis=dim, tiled=True)  85.9 us
    all_to_all x2, blocking collectives, sum_at_owner(): pieces = lax.all_to_all(split_up(x, dim, size), axis, 0, 0, tiled=True)  36.5 us
    dot_general x2, matrix products, update(): jnp.einsum('qhd,khd->hqk', queries[:, :, :plain_dim], key_rows, preferred...  29.7 us
    all_to_all x3, blocking collectives, sent_to_all(): return lax.all_to_all(copies, axis, split_axis=0, concat_axis=0, tiled=True)  27.6 us
    all_gather x1, waiting for transfers between devices, body(): lax.all_gather(down_weight, 'sp', axis=1, tiled=True)  27.4 us
    dot_general x2, matrix products, update(): jnp.einsum('hqk,khd->qhd', raised.astype(jnp.bfloat16), value_rows, prefe...  22.9 us
    reduce_sum x2, other arithmetic, update(): totals = totals * factor + jnp.sum(raised, axis=-1)  16.9 us
    dot_general x2, matrix products, update(): jnp.einsum('qhd,kd->hqk', queries[:, :, plain_dim:], rotary_rows, preferr...  16.2 us
  transfers between devices with their start and end apart: 3, of which 2 were waited for; matrix products, arithmetic and copies ran while one was open for 35% of the time, Pallas kernels for 0%

commit v1 on v0

v1 whole, which is shorter than its diff:
```python
import jax
import jax.numpy as jnp
from jax import lax
from jax.experimental import pallas as pl
from jax.experimental.pallas import tpu as pltpu
from jax.sharding import PartitionSpec as P

ROPE = 32
NOPE_A = 64
V_A = 64
NOPE_B = 128
V_B = 128
GRID_W = 64
EPS_ROOT = 1e-06
EPS_LAYER = 1e-05
THETA = 10000.0
DEEP_ALPHA = 2.0**0.25
LOG2E = 1.4426950408889634

NZ, NX, NY = 8, 4, 4
ROWS = 256
LAT = 256
DW = 512
D = 2048
FH = 1408
WB = 2 * FH
WA = FH
SLOT = 32
VD = V_A + V_B
KX = 128 + 256
C_A = (NOPE_A + ROPE) ** -0.5 * LOG2E
C_B = (NOPE_B + ROPE) ** -0.5 * LOG2E
MESH = pl.DeviceIdType.MESH
F32, BF16 = jnp.float32, jnp.bfloat16


def numbered(**counts):
    at, table = 0, {}
    for name, count in counts.items():
        table[name] = at
        at += count
    return table, at


M, MESSAGES = numbered(
    Q=6, KM=5, KP=4, KT=8, A1=4, AM=5, AP=4, BM=5, BP=4, XP=8, XM=8, RL=8, PW=8, O=4, OS=4,
    WO=6, AT=4, S1=4, G=5, F=4, S2=4,
)


def dot(a, b, dims):
    return lax.dot_general(a, b, (dims, ((), ())), preferred_element_type=F32)


def root_scale(latent, gain):
    x = latent.astype(F32)
    return x * lax.rsqrt(jnp.mean(x * x, axis=-1, keepdims=True) + EPS_ROOT) * gain


def turn(v, tab):
    cr, sr, cc, sc = tab[0:8], tab[8:16], tab[16:24], tab[24:32]
    a, b, c, d = v[0:8], v[8:16], v[16:24], v[24:32]
    return jnp.concatenate([a * cr - b * sr, b * cr + a * sr, c * cc - d * sc, d * cc + c * sc], axis=0)


def layer_kernel(
    res_ref, ql_ref, sl_ref, rk_ref, qg_ref, lg_ref, wqn_ref, kn_ref, vn_ref, wqw_ref, kw_ref,
    vw_ref, on_ref, ow_ref, g1_ref, b1_ref, gate_ref, up_ref, down_ref, g2_ref, b2_ref, tab_ref,
    out_ref,
    kvbuf, qbuf, wbuf, wk, wv, kx, vx, ml, acc, osend, orecv, srecv, att, wo, st1, sr1, st2, sr2,
    xbuf, gbuf, hid, fsend, frecv, hres, ss, rs, ls,
):
    s, t = lax.axis_index("sp"), lax.axis_index("tp")
    c = lax.rem(s, 2)
    x = lax.rem(lax.div(s, 2), NX)
    z = lax.div(s, 2 * NX)

    def at_z(off):
        return lax.rem(z + off + NZ, NZ)

    def at_x(off):
        return lax.rem(x + off + NX, NX)

    def at_y(off):
        return lax.rem(t + off + NY, NY)

    def dev_z(off):
        return (at_z(off) * (2 * NX) + x * 2 + c, t)

    def dev_x(off):
        return (z * (2 * NX) + at_x(off) * 2 + c, t)

    def dev_y(off):
        return (s, at_y(off))

    partner = (s + 1 - 2 * c, t)
    zz = lambda u: at_z(-u) if u <= 3 else at_z(u - 3)

    def msg(src, dst, i, dev):
        return pltpu.make_async_remote_copy(
            src_ref=src, dst_ref=dst, send_sem=ss.at[i], recv_sem=rs.at[i],
            device_id=dev, device_id_type=MESH,
        )

    def send(src, dst, i, dev):
        msg(src, dst, i, dev).start()

    def arrived(dst, i):
        msg(dst, dst, i, partner).wait_recv()

    def sent(src, i):
        msg(src, src, i, partner).wait_send()

    b_slot = lambda zi, xi: wbuf.at[zi, xi, c, :, 0:WB]
    a_slot = lambda zi, xi: wbuf.at[zi, xi, c, :, WB : WB + WA]
    a_row = lambda zi: wbuf.at[zi, :, c, :, WB : WB + WA]

    own = [
        pltpu.make_async_copy(gate_ref, wbuf.at[z, x, c, :, 0:FH], ls.at[0]),
        pltpu.make_async_copy(up_ref, wbuf.at[z, x, c, :, FH:WB], ls.at[1]),
        pltpu.make_async_copy(down_ref, wbuf.at[z, x, c, :, WB : WB + WA], ls.at[2]),
        pltpu.make_async_copy(on_ref.at[:, pl.ds(pl.multiple_of(t * DW, DW), DW)], wo.at[t, 0:V_A, :], ls.at[3]),
        pltpu.make_async_copy(ow_ref.at[:, pl.ds(pl.multiple_of(t * DW, DW), DW)], wo.at[t, V_A:VD, :], ls.at[4]),
    ]
    for o in own:
        o.start()

    barrier = pltpu.get_barrier_semaphore()
    friends = [dev_z(1), dev_z(-1), dev_x(1), dev_x(2), dev_x(3), partner, dev_y(1), dev_y(2), dev_y(3)]
    for f in friends:
        pl.semaphore_signal(barrier, inc=1, device_id=f, device_id_type=MESH)

    tab = tab_ref[...]
    kvbuf[z, c, 0:ROWS, :] = root_scale(sl_ref[...], lg_ref[...]).astype(BF16)
    kvbuf[z, c, ROWS : ROWS + ROPE, :] = turn(rk_ref[...].astype(F32), tab).astype(BF16)
    qn = root_scale(ql_ref[...], qg_ref[...]).astype(BF16)
    narrow = dot(wqn_ref[...], qn, ((1,), (1,)))
    wide = dot(wqw_ref[...], qn, ((1,), (1,)))
    qbuf[x, 0:96, :] = jnp.concatenate([narrow[0:NOPE_A], turn(narrow[NOPE_A:], tab)], axis=0).astype(BF16)
    qbuf[x, 224:384, :] = jnp.concatenate([turn(wide[NOPE_B:], tab), wide[0:NOPE_B]], axis=0).astype(BF16)
    for j in range(NX):
        qbuf[j, 96:224, :] = jnp.zeros((128, ROWS), BF16)
    wk[:, 0:64] = kn_ref[...]
    wk[:, 64:128] = jnp.zeros((LAT, 64), BF16)
    wk[:, 128:256] = kw_ref[...]
    wv[0:V_A, :] = vn_ref[...]
    wv[V_A:VD, :] = vw_ref[...]

    pl.semaphore_wait(barrier, len(friends))

    send(kvbuf.at[z, c], kvbuf.at[z, c], M["KM"] + 1, dev_z(-1))
    send(kvbuf.at[z, c], kvbuf.at[z, c], M["KP"] + 1, dev_z(1))
    send(kvbuf.at[z, c], kvbuf.at[z, c], M["KT"], partner)
    for j in (2, 1, 3):
        for half, rows in enumerate((slice(0, 96), slice(224, 384))):
            send(qbuf.at[x, rows, :], qbuf.at[x, rows, :], M["Q"] + (j - 1) * 2 + half, dev_x(j))
    for o in own[:3]:
        o.wait()
    for j in (2, 1, 3):
        send(a_slot(z, x), a_slot(z, x), M["A1"] + j, dev_x(j))
    send(b_slot(z, x), b_slot(z, x), M["BM"] + 1, dev_z(-1))
    send(b_slot(z, x), b_slot(z, x), M["BP"] + 1, dev_z(1))
    send(b_slot(z, x), b_slot(z, x), M["XP"], dev_x(1))
    send(b_slot(z, x), b_slot(z, x), M["XM"], dev_x(-1))
    for j in (2, 1, 3):
        cols = pl.ds(pl.multiple_of(at_y(j) * DW, DW), DW)
        send(on_ref.at[:, cols], wo.at[t, 0:V_A, :], M["WO"] + (j - 1) * 2, dev_y(j))
        send(ow_ref.at[:, cols], wo.at[t, V_A:VD, :], M["WO"] + (j - 1) * 2 + 1, dev_y(j))

    for j in range(NX):
        ml[j] = jnp.concatenate([jnp.full((2, ROWS), -jnp.inf, F32), jnp.zeros((6, ROWS), F32)], axis=0)
        acc[j] = jnp.zeros((VD, ROWS), F32)

    def keys_of(zs):
        lane = lax.broadcasted_iota(jnp.int32, (ROWS, 128), 1)
        for core in range(2):
            latent = kvbuf[zs, core, 0:ROWS, :]
            turned = kvbuf[zs, core, ROWS : ROWS + ROPE, :].astype(F32)
            rot = jnp.concatenate([jnp.zeros((64, ROWS), F32), turned, turned], axis=0).T
            keys = dot(latent, wk[...], ((1,), (0,)))
            at = slice(core * ROWS, (core + 1) * ROWS)
            kx[at, 0:128] = jnp.where(lane < 64, keys[:, 0:128], rot).astype(BF16)
            kx[at, 128:256] = rot.astype(BF16)
            kx[at, 256:384] = keys[:, 128:256].astype(BF16)
            vx[:, at] = dot(wv[...], latent, ((1,), (1,))).astype(BF16)

    def attend(zs):
        keys_of(zs)

        def per_rows(j, carry):
            for h, (lo, hi, vlo, vhi, scale) in enumerate(((0, 128, 0, V_A, C_A), (128, 384, V_A, VD, C_B))):
                scores = dot(kx[:, lo:hi], qbuf[j, lo:hi, :], ((1,), (0,)))
                old = ml[j, h : h + 1, :]
                new = jnp.maximum(old, jnp.max(scores, axis=0, keepdims=True))
                factor = jnp.exp2((old - new) * scale)
                raised = jnp.exp2((scores - new) * scale)
                ml[j, h : h + 1, :] = new
                ml[j, 2 + h : 3 + h, :] = ml[j, 2 + h : 3 + h, :] * factor + jnp.sum(raised, axis=0, keepdims=True)
                acc[j, vlo:vhi, :] = acc[j, vlo:vhi, :] * factor + dot(vx[vlo:vhi, :], raised.astype(BF16), ((1,), (0,)))
            return carry

        lax.fori_loop(0, NX, per_rows, 0)

    def step(k, carry):
        d = k + 1
        up_slot, low_slot = at_z(d), at_z(-d)
        arrived(kvbuf.at[up_slot, c], M["KM"] + d)

        @pl.when(d < 4)
        def _():
            send(kvbuf.at[up_slot, c], kvbuf.at[up_slot, c], M["KM"] + d + 1, dev_z(-1))

        send(kvbuf.at[up_slot, c], kvbuf.at[up_slot, c], M["KT"] + 3 + d, partner)

        @pl.when(d < 4)
        def _():
            arrived(kvbuf.at[low_slot, c], M["KP"] + d)

            @pl.when(d < 3)
            def _():
                send(kvbuf.at[low_slot, c], kvbuf.at[low_slot, c], M["KP"] + d + 1, dev_z(1))

            send(kvbuf.at[low_slot, c], kvbuf.at[low_slot, c], M["KT"] + d, partner)

        @pl.when(k == 0)
        def _():
            for j in range(1, NX):
                arrived(a_slot(z, at_x(-j)), M["A1"] + j)
            send(a_row(z), a_row(z), M["AM"] + 1, dev_z(-1))
            send(a_row(z), a_row(z), M["AP"] + 1, dev_z(1))
            for j in range(1, NX):
                for half, rows in enumerate((slice(0, 96), slice(224, 384))):
                    arrived(qbuf.at[at_x(-j), rows, :], M["Q"] + (j - 1) * 2 + half)

        arrived(kvbuf.at[at_z(-k), 1 - c], M["KT"] + k)
        attend(at_z(-k))

        arrived(b_slot(up_slot, x), M["BM"] + d)

        @pl.when(d < 4)
        def _():
            send(b_slot(up_slot, x), b_slot(up_slot, x), M["BM"] + d + 1, dev_z(-1))

        send(b_slot(up_slot, x), b_slot(up_slot, x), M["XP"] + 3 + d, dev_x(1))
        send(b_slot(up_slot, x), b_slot(up_slot, x), M["XM"] + 3 + d, dev_x(-1))

        @pl.when(d < 4)
        def _():
            arrived(b_slot(low_slot, x), M["BP"] + d)

            @pl.when(d < 3)
            def _():
                send(b_slot(low_slot, x), b_slot(low_slot, x), M["BP"] + d + 1, dev_z(1))

            send(b_slot(low_slot, x), b_slot(low_slot, x), M["XP"] + d, dev_x(1))
            send(b_slot(low_slot, x), b_slot(low_slot, x), M["XM"] + d, dev_x(-1))

        @pl.when(k > 0)
        def _():
            arrived(a_row(at_z(k)), M["AM"] + k)
            send(a_row(at_z(k)), a_row(at_z(k)), M["AM"] + k + 1, dev_z(-1))
            arrived(a_row(at_z(-k)), M["AP"] + k)

            @pl.when(k < 3)
            def _():
                send(a_row(at_z(-k)), a_row(at_z(-k)), M["AP"] + k + 1, dev_z(1))

        arrived(kvbuf.at[at_z(d), 1 - c], M["KT"] + 4 + k)
        attend(at_z(d))
        return carry

    lax.fori_loop(0, 4, step, 0)

    for j in range(NX):
        for h, (vlo, vhi) in enumerate(((0, V_A), (V_A, VD))):
            osend[j, vlo:vhi, :] = (acc[j, vlo:vhi, :] / ml[j, 2 + h : 3 + h, :]).astype(BF16)
    for j in (2, 1, 3):
        send(osend.at[at_x(j)], orecv.at[j - 1], M["O"] + j, dev_x(j))
        send(ml.at[at_x(j)], srecv.at[j - 1], M["OS"] + j, dev_x(j))

    def relay(u):
        zu = zz(u)
        arrived(b_slot(zu, at_x(-1)), M["XP"] + u)
        if u <= 3:
            send(b_slot(zu, at_x(-1)), b_slot(zu, at_x(-1)), M["RL"] + u, dev_x(1))
        arrived(b_slot(zu, at_x(1)), M["XM"] + u)
        if u > 3:
            send(b_slot(zu, at_x(1)), b_slot(zu, at_x(1)), M["RL"] + u, dev_x(-1))

    def across(u):
        arrived(b_slot(zz(u), at_x(2)), M["RL"] + u)
        send(wbuf.at[zz(u), :, c], wbuf.at[zz(u), :, c], M["PW"] + u, partner)

    for u in (0, 1, 4, 2, 5):
        relay(u)

    for j in range(1, NX):
        arrived(orecv.at[j - 1], M["O"] + j)
        arrived(srecv.at[j - 1], M["OS"] + j)
    for h, (vlo, vhi, scale) in enumerate(((0, V_A, C_A), (V_A, VD, C_B))):
        tops = [ml[x, h : h + 1, :]] + [srecv[j, h : h + 1, :] for j in range(3)]
        sums = [ml[x, 2 + h : 3 + h, :]] + [srecv[j, 2 + h : 3 + h, :] for j in range(3)]
        parts = [osend[x, vlo:vhi, :]] + [orecv[j, vlo:vhi, :] for j in range(3)]
        top = jnp.maximum(jnp.maximum(tops[0], tops[1]), jnp.maximum(tops[2], tops[3]))
        shares = [total * jnp.exp2((m - top) * scale) for m, total in zip(tops, sums)]
        total = shares[0] + shares[1] + shares[2] + shares[3]
        mixed = sum(part.astype(F32) * (share / total) for part, share in zip(parts, shares))
        att[t, vlo:vhi, :] = mixed.astype(BF16)
    for j in (2, 1, 3):
        send(att.at[t], att.at[t], M["AT"] + j, dev_y(j))

    for u in (3, 6, 7):
        relay(u)
    arrived(a_row(at_z(4)), M["AM"] + 4)
    for u in (0, 1, 4):
        across(u)

    for o in own[3:]:
        o.wait()
    for j in range(1, NY):
        for half, rows in enumerate((slice(0, V_A), slice(V_A, VD))):
            arrived(wo.at[at_y(-j), rows, :], M["WO"] + (j - 1) * 2 + half)
    for j in range(1, NY):
        arrived(att.at[at_y(-j)], M["AT"] + j)

    def norm(stat, got, first, gain_ref, bias_ref):
        h = hres[...]
        center = jnp.mean(h, axis=1, keepdims=True)
        apart = jnp.sum((h - center) * (h - center), axis=1, keepdims=True)
        lane = lax.broadcasted_iota(jnp.int32, (ROWS, 128), 1)
        both = jnp.where(lane == 0, center, jnp.where(lane == 1, apart, 0.0))
        stat[...] = both.T[0:8]
        for j in (2, 1, 3):
            send(stat, got.at[j - 1], first + j, dev_y(j))
        for j in range(1, NY):
            arrived(got.at[j - 1], first + j)
        centers = [stat[0:1, :]] + [got[j, 0:1, :] for j in range(3)]
        aparts = [stat[1:2, :]] + [got[j, 1:2, :] for j in range(3)]
        middle = (centers[0] + centers[1] + centers[2] + centers[3]) * 0.25
        spread = sum(aparts) + DW * sum((m - middle) * (m - middle) for m in centers)
        root = lax.rsqrt(spread * (1.0 / D) + EPS_LAYER)
        cols = jnp.concatenate([middle, root, jnp.zeros((126, ROWS), F32)], axis=0).T
        return ((h - cols[:, 0:1]) * cols[:, 1:2] * gain_ref[...] + bias_ref[...]).astype(BF16)

    mixed = dot(att[...].reshape(NY * VD, ROWS), wo[...].reshape(NY * VD, DW), ((0,), (0,)))
    hres[...] = DEEP_ALPHA * res_ref[...].astype(F32) + mixed
    mine = pl.ds(pl.multiple_of(t * DW, DW), DW)
    normed = norm(st1, sr1, M["S1"], g1_ref, b1_ref)
    xbuf[:, mine] = normed
    hres[...] = DEEP_ALPHA * normed.astype(F32)

    x_part = lambda off, rows: xbuf.at[rows, pl.ds(pl.multiple_of(at_y(off) * DW, DW), DW)]
    every, first_half, second_half = slice(0, ROWS), slice(0, ROWS // 2), slice(ROWS // 2, ROWS)
    send(x_part(0, every), x_part(0, every), M["G"] + 1, dev_y(1))
    send(x_part(0, every), x_part(0, every), M["G"] + 2, dev_y(-1))
    for u in (2, 5):
        across(u)
    arrived(x_part(-1, every), M["G"] + 1)
    send(x_part(-1, first_half), x_part(-1, first_half), M["G"] + 3, dev_y(1))
    arrived(x_part(1, every), M["G"] + 2)
    send(x_part(1, second_half), x_part(1, second_half), M["G"] + 4, dev_y(-1))
    for u in (3, 6, 7):
        across(u)
    arrived(x_part(2, first_half), M["G"] + 3)
    arrived(x_part(2, second_half), M["G"] + 4)
    for u in range(NZ):
        arrived(wbuf.at[zz(u), :, 1 - c], M["PW"] + u)

    def gate_up(n, carry):
        cols = pl.ds(pl.multiple_of(n * 256, 256), 256)
        gbuf[:, cols] = dot(xbuf[...], wbuf[:, :, :, :, cols].reshape(D, 256), ((1,), (0,)))
        return carry

    lax.fori_loop(0, WB // 256, gate_up, 0)
    gate = gbuf[:, 0:FH]
    hid[...] = (gate / (1.0 + jnp.exp(-gate)) * gbuf[:, FH:WB]).astype(BF16)

    def feed(off):
        return dot(hid[...], wbuf[pl.ds(at_y(off) * 2, 2), :, :, :, WB : WB + WA].reshape(DW, FH), ((1,), (1,)))

    for j in (2, 1, 3):
        fsend[j - 1] = feed(j).astype(BF16)
        send(fsend.at[j - 1], frecv.at[j - 1], M["F"] + j, dev_y(j))
    hres[...] += feed(0)
    for j in range(1, NY):
        arrived(frecv.at[j - 1], M["F"] + j)
    hres[...] += frecv[0].astype(F32) + frecv[1].astype(F32) + frecv[2].astype(F32)
    out_ref[...] = norm(st2, sr2, M["S2"], g2_ref, b2_ref)

    for j in range(1, NX):
        sent(qbuf.at[0, 0:96, :], M["Q"] + (j - 1) * 2)
        sent(qbuf.at[0, 224:384, :], M["Q"] + (j - 1) * 2 + 1)
        sent(a_slot(0, 0), M["A1"] + j)
        sent(osend.at[0], M["O"] + j)
        sent(ml.at[0], M["OS"] + j)
        sent(wo.at[0, 0:V_A, :], M["WO"] + (j - 1) * 2)
        sent(wo.at[0, V_A:VD, :], M["WO"] + (j - 1) * 2 + 1)
        sent(att.at[0], M["AT"] + j)
        sent(st1, M["S1"] + j)
        sent(fsend.at[0], M["F"] + j)
        sent(st2, M["S2"] + j)
    for d in range(1, 5):
        for name, ref in (("K", kvbuf.at[0, 0]), ("A", a_row(0)), ("B", b_slot(0, 0))):
            sent(ref, M[name + "M"] + d)
            if d < 4:
                sent(ref, M[name + "P"] + d)
    for u in range(NZ):
        sent(kvbuf.at[0, 0], M["KT"] + u)
        sent(b_slot(0, 0), M["XP"] + u)
        sent(b_slot(0, 0), M["XM"] + u)
        sent(b_slot(0, 0), M["RL"] + u)
        sent(wbuf.at[0, :, c], M["PW"] + u)
    for i in (1, 2):
        sent(x_part(0, every), M["G"] + i)
        sent(x_part(0, first_half), M["G"] + 2 + i)


def body(
    residual, query_latent, shared_latent, rotary_key, query_gain, latent_gain, query_narrow, key_narrow,
    value_narrow, query_wide, key_wide, value_wide, output_narrow, output_wide, first_gain, first_bias,
    gate_weight, up_weight, down_weight, second_gain, second_bias,
):
    positions = lax.axis_index("sp") * ROWS + jnp.arange(ROWS, dtype=jnp.int32)
    quarter = ROPE // 4
    freqs = THETA ** (-(2.0 * jnp.arange(quarter, dtype=F32)) / (2 * quarter))
    row_angle = freqs[:, None] * (positions // GRID_W).astype(F32)[None, :]
    col_angle = freqs[:, None] * (positions % GRID_W).astype(F32)[None, :]
    tab = jnp.concatenate([jnp.cos(row_angle), jnp.sin(row_angle), jnp.cos(col_angle), jnp.sin(col_angle)], axis=0)
    row = lambda v: v.reshape(1, -1)
    operands = (
        residual, query_latent, shared_latent, rotary_key.T, row(query_gain), row(latent_gain), query_narrow.T,
        key_narrow, value_narrow.T, query_wide.T, key_wide, value_wide.T, output_narrow, output_wide,
        row(first_gain), row(first_bias), gate_weight, up_weight, down_weight.T, row(second_gain),
        row(second_bias), tab,
    )
    vmem = pl.BlockSpec(memory_space=pltpu.VMEM)
    return pl.pallas_call(
        layer_kernel,
        out_shape=jax.ShapeDtypeStruct((ROWS, DW), BF16),
        in_specs=[vmem] * len(operands),
        out_specs=vmem,
        scratch_shapes=[
            pltpu.VMEM((NZ, 2, ROWS + ROPE, LAT), BF16),
            pltpu.VMEM((NX, KX, ROWS), BF16),
            pltpu.VMEM((NZ, NX, 2, SLOT, WB + WA), BF16),
            pltpu.VMEM((LAT, 256), BF16),
            pltpu.VMEM((VD, LAT), BF16),
            pltpu.VMEM((2 * ROWS, KX), BF16),
            pltpu.VMEM((VD, 2 * ROWS), BF16),
            pltpu.VMEM((NX, 8, ROWS), F32),
            pltpu.VMEM((NX, VD, ROWS), F32),
            pltpu.VMEM((NX, VD, ROWS), BF16),
            pltpu.VMEM((3, VD, ROWS), BF16),
            pltpu.VMEM((3, 8, ROWS), F32),
            pltpu.VMEM((NY, VD, ROWS), BF16),
            pltpu.VMEM((NY, VD, DW), BF16),
            pltpu.VMEM((8, ROWS), F32),
            pltpu.VMEM((3, 8, ROWS), F32),
            pltpu.VMEM((8, ROWS), F32),
            pltpu.VMEM((3, 8, ROWS), F32),
            pltpu.VMEM((ROWS, D), BF16),
            pltpu.VMEM((ROWS, WB), F32),
            pltpu.VMEM((ROWS, FH), BF16),
            pltpu.VMEM((3, ROWS, DW), BF16),
            pltpu.VMEM((3, ROWS, DW), BF16),
            pltpu.VMEM((ROWS, DW), F32),
            pltpu.SemaphoreType.DMA((MESSAGES,)),
            pltpu.SemaphoreType.DMA((MESSAGES,)),
            pltpu.SemaphoreType.DMA((5,)),
        ],
        compiler_params=pltpu.CompilerParams(
            collective_id=0, has_side_effects=True, vmem_limit_bytes=60 * 1024 * 1024
        ),
    )(*operands)


def solution(mesh):
    return jax.shard_map(
        body,
        mesh=mesh,
        in_specs=(
            P("sp", "tp"),
            P("sp", None),
            P("sp", None),
            P("sp", None),
            P(),
            P(),
            P(None, "tp"),
            P(None, "tp"),
            P(None, "tp"),
            P(None, "tp"),
            P(None, "tp"),
            P(None, "tp"),
            P("tp", None),
            P("tp", None),
            P("tp"),
            P("tp"),
            P("sp", "tp"),
            P("sp", "tp"),
            P("tp", "sp"),
            P("tp"),
            P("tp"),
        ),
        out_specs=P("sp", "tp"),
        check_vma=False,
    )
```

time: 314 us -> 128 us (0.41)
  Pallas kernels: 0 us -> 122 us
  waiting for transfers between devices: 114 us -> 0 us
  matrix products: 86.3 us -> 0 us
  blocking collectives: 64.1 us -> 0 us
  other arithmetic: 33.9 us -> 0.77 us
  between operations: 13.4 us -> 0.04 us
    pallas_call x0 -> x1, Pallas kernels: none -> 122 us  [body(): pl.pallas_call(layer_kernel, out_shape=jax.ShapeDtypeStruct((ROWS, DW), B...]
    all_gather x3 -> x0, waiting for transfers between devices: 113 us -> none  [the longest x2 85.9 us: in_one_piece(): lax.all_gather(both, axis, axis=dim, tiled=True)]
    dot_general x12 -> x0, matrix products: 86.3 us -> none  [the longest x2 29.7 us: update(): jnp.einsum('qhd,khd->hqk', queries[:, :, :plain_dim], key_rows, preferred...]
    all_to_all x5 -> x0, blocking collectives: 64.1 us -> none  [the longest x2 36.5 us: sum_at_owner(): pieces = lax.all_to_all(split_up(x, dim, size), axis, 0, 0, tiled=True)]
    reduce_sum x10 -> x0, other arithmetic: 23.8 us -> none  [the longest x2 16.9 us: update(): totals = totals * factor + jnp.sum(raised, axis=-1)]
    concatenate x5 -> x1, other arithmetic: 7.39 us -> 0.6 us  [body(): jnp.concatenate([jnp.cos(row_angle), jnp.sin(row_angle), jnp.cos(col_angl...]
  transfers between devices with their start and end apart: 3 -> 0, of which waited for: 2 -> 0; matrix products, arithmetic and copies ran while one was open for 35% -> 0% of each run, Pallas kernels for 0% -> 0%
where the time goes in v1:
time: 128 us; the launch traced here: 126 us
  Pallas kernels  122 us (95%)
  local copies, waits for them, and re-layouts  3.29 us (3%)
    pallas_call x1, Pallas kernels, body(): pl.pallas_call(layer_kernel, out_shape=jax.ShapeDtypeStruct((ROWS, DW), B...  122 us
    unnamed x7, local copies, waits for them, and re-layouts  3.29 us

profile of v1, /device:TPU:1, one launch (start us, length us, event | category | flops | bytes accessed | tf_op | source)
XLA Modules:
  0.0 126.4 jit_solution(9257907431070290504)
XLA Ops:
  0.0 0.1 multiply_cosine_fusion.1
  0.2 0.0 copy-start.1
  0.2 0.0 copy-start
  0.2 0.6 pad_maximum_fusion.tab_ref
  0.8 0.1 copy-done.1
  0.9 0.7 copy.23.kn_ref
  1.7 0.0 copy-done
  1.7 0.7 copy.22
  2.4 122.3 %shard_map.199 = bf16[256,512]{1,0:T(8,128)(2,1)} custom-call(bf16[256,512]{1,0:T(8,128)(2,1)} %res_ref.1, bf16[256,512]{1,0:T(8,128)(2,1)} %ql_ref.1, bf16[256,256]{1,0:T(8,128)(2,1)} %sl_ref.1, bf16[32,256]{1,0:T(8,128)(2,1)} %bitcast.17, f32[1,512]{1,0:T(1,128)} %bitcast.18, f32[1,256]{1,0:T(1,128)} %bitcast.23, bf16[96,512]{1,0:T(8,128)(2,1)} %bitcast.14, ...), custom_call_target="tpu_custom_call" | custom-call | tf_op jit(solution)/shard_map/pallas_call | solution.py:437
  124.8 1.7 %copy.25 = bf16[256,512]{1,0:T(8,128)(2,1)} copy(bf16[256,512]{1,0:T(8,128)(2,1)} %shard_map.199) | data formatting | bytes 524288
  (2 shorter events, 0.0 us)
Async XLA Ops:
  0.2 0.8 copy-start.1
  0.2 1.5 %copy-start = (bf16[256,128]{1,0:T(8,128)(2,1)S(1)}, bf16[256,128]{1,0:T(8,128)(2,1)}, u32[]{:S(2)}) copy-start(bf16[256,128]{1,0:T(8,128)(2,1)} %param.32) | copy-start | bytes 196612

commit v2 on v1

--- a/solution.py
+++ b/solution.py
@@ -23,8 +23,9 @@
 DW = 512
 D = 2048
 FH = 1408
-WB = 2 * FH
-WA = FH
+GU = 2 * FH
+WT = 3 * FH
+WB = GU - 256
 SLOT = 32
 VD = V_A + V_B
 KX = 128 + 256
@@ -43,8 +44,8 @@
 
 
 M, MESSAGES = numbered(
-    Q=6, KM=5, KP=4, KT=8, A1=4, AM=5, AP=4, BM=5, BP=4, XP=8, XM=8, RL=8, PW=8, O=4, OS=4,
-    WO=6, AT=4, S1=4, G=5, F=4, S2=4,
+    Q=6, KM=5, KP=4, KT=8, A1=4, AM=4, AP=5, BM=5, BP=4, XP=8, XM=8, RL=8, PB=32, PA=8, O=4, OS=4,
+    WO=6, AT=4, S1=4, G=4, F=4, S2=4,
 )
 
 
@@ -58,14 +59,14 @@
 
 
 def turn(v, tab):
-    cr, sr, cc, sc = tab[0:8], tab[8:16], tab[16:24], tab[24:32]
+    cr, sr, cc, sc = tab
     a, b, c, d = v[0:8], v[8:16], v[16:24], v[24:32]
     return jnp.concatenate([a * cr - b * sr, b * cr + a * sr, c * cc - d * sc, d * cc + c * sc], axis=0)
 
 
 def layer_kernel(
     res_ref, ql_ref, sl_ref, rk_ref, qg_ref, lg_ref, wqn_ref, kn_ref, vn_ref, wqw_ref, kw_ref,
-    vw_ref, on_ref, ow_ref, g1_ref, b1_ref, gate_ref, up_ref, down_ref, g2_ref, b2_ref, tab_ref,
+    vw_ref, on_ref, ow_ref, g1_ref, b1_ref, gate_ref, up_ref, down_ref, g2_ref, b2_ref, cr_ref, sr_ref, cc_ref, sc_ref,
     out_ref,
     kvbuf, qbuf, wbuf, wk, wv, kx, vx, ml, acc, osend, orecv, srecv, att, wo, st1, sr1, st2, sr2,
     xbuf, gbuf, hid, fsend, frecv, hres, ss, rs, ls,
@@ -94,7 +95,10 @@
         return (s, at_y(off))
 
     partner = (s + 1 - 2 * c, t)
-    zz = lambda u: at_z(-u) if u <= 3 else at_z(u - 3)
+
+    def zz(u):
+        return at_z(lax.div(u + 1, 2) * (1 - 2 * lax.rem(u, 2)) if not isinstance(u, int) else (u + 1) // 2 * (1 - 2 * (u % 2)))
+
 
     def msg(src, dst, i, dev):
         return pltpu.make_async_remote_copy(
@@ -112,13 +116,13 @@
         msg(src, src, i, partner).wait_send()
 
     b_slot = lambda zi, xi: wbuf.at[zi, xi, c, :, 0:WB]
-    a_slot = lambda zi, xi: wbuf.at[zi, xi, c, :, WB : WB + WA]
-    a_row = lambda zi: wbuf.at[zi, :, c, :, WB : WB + WA]
+    a_slot = lambda zi, xi: wbuf.at[zi, xi, c, :, WB:WT]
+    a_row = lambda zi: wbuf.at[zi, :, c, :, WB:WT]
 
     own = [
         pltpu.make_async_copy(gate_ref, wbuf.at[z, x, c, :, 0:FH], ls.at[0]),
-        pltpu.make_async_copy(up_ref, wbuf.at[z, x, c, :, FH:WB], ls.at[1]),
-        pltpu.make_async_copy(down_ref, wbuf.at[z, x, c, :, WB : WB + WA], ls.at[2]),
+        pltpu.make_async_copy(up_ref, wbuf.at[z, x, c, :, FH:GU], ls.at[1]),
+        pltpu.make_async_copy(down_ref, wbuf.at[z, x, c, :, GU:WT], ls.at[2]),
         pltpu.make_async_copy(on_ref.at[:, pl.ds(pl.multiple_of(t * DW, DW), DW)], wo.at[t, 0:V_A, :], ls.at[3]),
         pltpu.make_async_copy(ow_ref.at[:, pl.ds(pl.multiple_of(t * DW, DW), DW)], wo.at[t, V_A:VD, :], ls.at[4]),
     ]
@@ -130,7 +134,7 @@
     for f in friends:
         pl.semaphore_signal(barrier, inc=1, device_id=f, device_id_type=MESH)
 
-    tab = tab_ref[...]
+    tab = (cr_ref[...], sr_ref[...], cc_ref[...], sc_ref[...])
     kvbuf[z, c, 0:ROWS, :] = root_scale(sl_ref[...], lg_ref[...]).astype(BF16)
     kvbuf[z, c, ROWS : ROWS + ROPE, :] = turn(rk_ref[...].astype(F32), tab).astype(BF16)
     qn = root_scale(ql_ref[...], qg_ref[...]).astype(BF16)
@@ -140,11 +144,11 @@
     qbuf[x, 224:384, :] = jnp.concatenate([turn(wide[NOPE_B:], tab), wide[0:NOPE_B]], axis=0).astype(BF16)
     for j in range(NX):
         qbuf[j, 96:224, :] = jnp.zeros((128, ROWS), BF16)
-    wk[:, 0:64] = kn_ref[...]
+    wk[:, 0:64] = kn_ref[...].T
     wk[:, 64:128] = jnp.zeros((LAT, 64), BF16)
     wk[:, 128:256] = kw_ref[...]
     wv[0:V_A, :] = vn_ref[...]
-    wv[V_A:VD, :] = vw_ref[...]
+    wv[V_A:VD, :] = vw_ref[...].T
 
     pl.semaphore_wait(barrier, len(friends))
 
@@ -162,6 +166,7 @@
     send(b_slot(z, x), b_slot(z, x), M["BP"] + 1, dev_z(1))
     send(b_slot(z, x), b_slot(z, x), M["XP"], dev_x(1))
     send(b_slot(z, x), b_slot(z, x), M["XM"], dev_x(-1))
+    send(b_slot(z, x), b_slot(z, x), M["PB"], partner)
     for j in (2, 1, 3):
         cols = pl.ds(pl.multiple_of(at_y(j) * DW, DW), DW)
         send(on_ref.at[:, cols], wo.at[t, 0:V_A, :], M["WO"] + (j - 1) * 2, dev_y(j))
@@ -187,9 +192,13 @@
     def attend(zs):
         keys_of(zs)
 
-        def per_rows(j, carry):
-            for h, (lo, hi, vlo, vhi, scale) in enumerate(((0, 128, 0, V_A, C_A), (128, 384, V_A, VD, C_B))):
-                scores = dot(kx[:, lo:hi], qbuf[j, lo:hi, :], ((1,), (0,)))
+        heads = ((0, 128, 0, V_A, C_A), (128, 384, V_A, VD, C_B))
+        every_score = [
+            [dot(kx[:, lo:hi], qbuf[j, lo:hi, :], ((1,), (0,))) for lo, hi, _, _, _ in heads] for j in range(NX)
+        ]
+        for j in range(NX):
+            for h, (_, _, vlo, vhi, scale) in enumerate(heads):
+                scores = every_score[j][h]
                 old = ml[j, h : h + 1, :]
                 new = jnp.maximum(old, jnp.max(scores, axis=0, keepdims=True))
                 factor = jnp.exp2((old - new) * scale)
@@ -197,12 +206,22 @@
                 ml[j, h : h + 1, :] = new
                 ml[j, 2 + h : 3 + h, :] = ml[j, 2 + h : 3 + h, :] * factor + jnp.sum(raised, axis=0, keepdims=True)
                 acc[j, vlo:vhi, :] = acc[j, vlo:vhi, :] * factor + dot(vx[vlo:vhi, :], raised.astype(BF16), ((1,), (0,)))
-            return carry
-
-        lax.fori_loop(0, NX, per_rows, 0)
+
+    def to_partner(u, zi, way):
+        xi = at_x((0, -1, 1, 2)[way])
+        send(b_slot(zi, xi), b_slot(zi, xi), M["PB"] + 4 * u + way, partner)
+
+    def row_to_partner(u, zi):
+        send(a_row(zi), a_row(zi), M["PA"] + u, partner)
+
+    def to_x(u, zi):
+        send(b_slot(zi, x), b_slot(zi, x), M["XP"] + u, dev_x(1))
+        send(b_slot(zi, x), b_slot(zi, x), M["XM"] + u, dev_x(-1))
 
     def step(k, carry):
         d = k + 1
+        u1 = 2 * k - lax.div(k + 3, 4)
+        low, up = 2 * d - 1, 2 * d - lax.div(d, 4)
         up_slot, low_slot = at_z(d), at_z(-d)
         arrived(kvbuf.at[up_slot, c], M["KM"] + d)
 
@@ -210,7 +229,7 @@
         def _():
             send(kvbuf.at[up_slot, c], kvbuf.at[up_slot, c], M["KM"] + d + 1, dev_z(-1))
 
-        send(kvbuf.at[up_slot, c], kvbuf.at[up_slot, c], M["KT"] + 3 + d, partner)
+        send(kvbuf.at[up_slot, c], kvbuf.at[up_slot, c], M["KT"] + up, partner)
 
         @pl.when(d < 4)
         def _():
@@ -220,52 +239,47 @@
             def _():
                 send(kvbuf.at[low_slot, c], kvbuf.at[low_slot, c], M["KP"] + d + 1, dev_z(1))
 
-            send(kvbuf.at[low_slot, c], kvbuf.at[low_slot, c], M["KT"] + d, partner)
+            send(kvbuf.at[low_slot, c], kvbuf.at[low_slot, c], M["KT"] + low, partner)
 
         @pl.when(k == 0)
+        def _():
+            for j in range(1, NX):
+                for half, rows in enumerate((slice(0, 96), slice(224, 384))):
+                    arrived(qbuf.at[at_x(-j), rows, :], M["Q"] + (j - 1) * 2 + half)
+
+        arrived(kvbuf.at[at_z(-k), 1 - c], M["KT"] + u1)
+        attend(at_z(-k))
+
+        arrived(b_slot(up_slot, x), M["BM"] + d)
+        to_partner(up, up_slot, 0)
+
+        @pl.when(d < 4)
+        def _():
+            send(b_slot(up_slot, x), b_slot(up_slot, x), M["BM"] + d + 1, dev_z(-1))
+
+        @pl.when(d < 3)
+        def _():
+            to_x(up, up_slot)
+
+        @pl.when(d < 4)
+        def _():
+            arrived(b_slot(low_slot, x), M["BP"] + d)
+            to_partner(low, low_slot, 0)
+
+            @pl.when(d < 3)
+            def _():
+                send(b_slot(low_slot, x), b_slot(low_slot, x), M["BP"] + d + 1, dev_z(1))
+                to_x(low, low_slot)
+
+        @pl.when(k == 2)
         def _():
             for j in range(1, NX):
                 arrived(a_slot(z, at_x(-j)), M["A1"] + j)
             send(a_row(z), a_row(z), M["AM"] + 1, dev_z(-1))
             send(a_row(z), a_row(z), M["AP"] + 1, dev_z(1))
-            for j in range(1, NX):
-                for half, rows in enumerate((slice(0, 96), slice(224, 384))):
-                    arrived(qbuf.at[at_x(-j), rows, :], M["Q"] + (j - 1) * 2 + half)
-
-        arrived(kvbuf.at[at_z(-k), 1 - c], M["KT"] + k)
-        attend(at_z(-k))
-
-        arrived(b_slot(up_slot, x), M["BM"] + d)
-
-        @pl.when(d < 4)
-        def _():
-            send(b_slot(up_slot, x), b_slot(up_slot, x), M["BM"] + d + 1, dev_z(-1))
-
-        send(b_slot(up_slot, x), b_slot(up_slot, x), M["XP"] + 3 + d, dev_x(1))
-        send(b_slot(up_slot, x), b_slot(up_slot, x), M["XM"] + 3 + d, dev_x(-1))
-
-        @pl.when(d < 4)
-        def _():
-            arrived(b_slot(low_slot, x), M["BP"] + d)
-
-            @pl.when(d < 3)
-            def _():
-                send(b_slot(low_slot, x), b_slot(low_slot, x), M["BP"] + d + 1, dev_z(1))
-
-            send(b_slot(low_slot, x), b_slot(low_slot, x), M["XP"] + d, dev_x(1))
-            send(b_slot(low_slot, x), b_slot(low_slot, x), M["XM"] + d, dev_x(-1))
-
-        @pl.when(k > 0)
-        def _():
-            arrived(a_row(at_z(k)), M["AM"] + k)
-            send(a_row(at_z(k)), a_row(at_z(k)), M["AM"] + k + 1, dev_z(-1))
-            arrived(a_row(at_z(-k)), M["AP"] + k)
-
-            @pl.when(k < 3)
-            def _():
-                send(a_row(at_z(-k)), a_row(at_z(-k)), M["AP"] + k + 1, dev_z(1))
-
-        arrived(kvbuf.at[at_z(d), 1 - c], M["KT"] + 4 + k)
+            row_to_partner(0, z)
+
+        arrived(kvbuf.at[at_z(d), 1 - c], M["KT"] + up)
         attend(at_z(d))
         return carry
 
@@ -278,21 +292,40 @@
         send(osend.at[at_x(j)], orecv.at[j - 1], M["O"] + j, dev_x(j))
         send(ml.at[at_x(j)], srecv.at[j - 1], M["OS"] + j, dev_x(j))
 
+    for u in (5, 6, 7):
+        to_x(u, zz(u))
+
+    plus = (0, 1, 3, 5)
+
     def relay(u):
         zu = zz(u)
         arrived(b_slot(zu, at_x(-1)), M["XP"] + u)
-        if u <= 3:
+        if u in plus:
             send(b_slot(zu, at_x(-1)), b_slot(zu, at_x(-1)), M["RL"] + u, dev_x(1))
+        to_partner(u, zu, 1)
         arrived(b_slot(zu, at_x(1)), M["XM"] + u)
-        if u > 3:
+        if u not in plus:
             send(b_slot(zu, at_x(1)), b_slot(zu, at_x(1)), M["RL"] + u, dev_x(-1))
+        to_partner(u, zu, 2)
 
     def across(u):
         arrived(b_slot(zz(u), at_x(2)), M["RL"] + u)
-        send(wbuf.at[zz(u), :, c], wbuf.at[zz(u), :, c], M["PW"] + u, partner)
-
-    for u in (0, 1, 4, 2, 5):
-        relay(u)
+        to_partner(u, zz(u), 3)
+
+    def rows_round(d):
+        arrived(a_row(at_z(-d)), M["AP"] + d)
+        if d < 4:
+            send(a_row(at_z(-d)), a_row(at_z(-d)), M["AP"] + d + 1, dev_z(1))
+        row_to_partner(2 * d - 1, at_z(-d))
+        if d < 4:
+            arrived(a_row(at_z(d)), M["AM"] + d)
+            if d < 3:
+                send(a_row(at_z(d)), a_row(at_z(d)), M["AM"] + d + 1, dev_z(-1))
+            row_to_partner(2 * d, at_z(d))
+
+    relay(0)
+    relay(1)
+    rows_round(1)
 
     for j in range(1, NX):
         arrived(orecv.at[j - 1], M["O"] + j)
@@ -309,11 +342,8 @@
     for j in (2, 1, 3):
         send(att.at[t], att.at[t], M["AT"] + j, dev_y(j))
 
-    for u in (3, 6, 7):
-        relay(u)
-    arrived(a_row(at_z(4)), M["AM"] + 4)
-    for u in (0, 1, 4):
-        across(u)
+    relay(2)
+    relay(3)
 
     for o in own[3:]:
         o.wait()
@@ -323,7 +353,7 @@
     for j in range(1, NY):
         arrived(att.at[at_y(-j)], M["AT"] + j)
 
-    def norm(stat, got, first, gain_ref, bias_ref):
+    def norm(stat, got, first, gain_ref, bias_ref, between):
         h = hres[...]
         center = jnp.mean(h, axis=1, keepdims=True)
         apart = jnp.sum((h - center) * (h - center), axis=1, keepdims=True)
@@ -332,6 +362,7 @@
         stat[...] = both.T[0:8]
         for j in (2, 1, 3):
             send(stat, got.at[j - 1], first + j, dev_y(j))
+        between()
         for j in range(1, NY):
             arrived(got.at[j - 1], first + j)
         centers = [stat[0:1, :]] + [got[j, 0:1, :] for j in range(3)]
@@ -345,38 +376,58 @@
     mixed = dot(att[...].reshape(NY * VD, ROWS), wo[...].reshape(NY * VD, DW), ((0,), (0,)))
     hres[...] = DEEP_ALPHA * res_ref[...].astype(F32) + mixed
     mine = pl.ds(pl.multiple_of(t * DW, DW), DW)
-    normed = norm(st1, sr1, M["S1"], g1_ref, b1_ref)
+    normed = norm(st1, sr1, M["S1"], g1_ref, b1_ref, lambda: (rows_round(2), relay(4)))
     xbuf[:, mine] = normed
     hres[...] = DEEP_ALPHA * normed.astype(F32)
 
-    x_part = lambda off, rows: xbuf.at[rows, pl.ds(pl.multiple_of(at_y(off) * DW, DW), DW)]
-    every, first_half, second_half = slice(0, ROWS), slice(0, ROWS // 2), slice(ROWS // 2, ROWS)
-    send(x_part(0, every), x_part(0, every), M["G"] + 1, dev_y(1))
-    send(x_part(0, every), x_part(0, every), M["G"] + 2, dev_y(-1))
-    for u in (2, 5):
-        across(u)
-    arrived(x_part(-1, every), M["G"] + 1)
-    send(x_part(-1, first_half), x_part(-1, first_half), M["G"] + 3, dev_y(1))
-    arrived(x_part(1, every), M["G"] + 2)
-    send(x_part(1, second_half), x_part(1, second_half), M["G"] + 4, dev_y(-1))
-    for u in (3, 6, 7):
-        across(u)
-    arrived(x_part(2, first_half), M["G"] + 3)
-    arrived(x_part(2, second_half), M["G"] + 4)
+    x_part = lambda off: xbuf.at[:, pl.ds(pl.multiple_of(at_y(off) * DW, DW), DW)]
+    for j in (2, 1, 3):
+        send(x_part(0), x_part(0), M["G"] + j, dev_y(j))
+    across(0)
+    across(1)
+    relay(5)
+    across(2)
+    rows_round(3)
+    relay(6)
+    across(3)
+    relay(7)
+    for j in range(1, NY):
+        arrived(x_part(-j), M["G"] + j)
+
+    def gate_up(u):
+        zu = zz(u)
+        features = xbuf[:, pl.ds(pl.multiple_of(zu * 256, 256), 256)]
+        for n in range(WB // 256):
+            cols = slice(n * 256, (n + 1) * 256)
+            part = dot(features, wbuf[zu, :, :, :, cols].reshape(256, 256), ((1,), (0,)))
+            gbuf[:, cols] = part if isinstance(u, int) else gbuf[:, cols] + part
+
+    def partner_block(u):
+        for way in range(4):
+            arrived(wbuf.at[zz(u), at_x((0, -1, 1, 2)[way]), 1 - c, :, 0:WB], M["PB"] + 4 * u + way)
+
+    partner_block(0)
+    gate_up(0)
+
+    def block(u, carry):
+        @pl.when(u <= 4)
+        def _():
+            across(u + 3)
+
+        partner_block(u)
+        gate_up(u)
+        return carry
+
+    lax.fori_loop(1, NZ, block, 0)
+    rows_round(4)
     for u in range(NZ):
-        arrived(wbuf.at[zz(u), :, 1 - c], M["PW"] + u)
-
-    def gate_up(n, carry):
-        cols = pl.ds(pl.multiple_of(n * 256, 256), 256)
-        gbuf[:, cols] = dot(xbuf[...], wbuf[:, :, :, :, cols].reshape(D, 256), ((1,), (0,)))
-        return carry
-
-    lax.fori_loop(0, WB // 256, gate_up, 0)
+        arrived(wbuf.at[zz(u), :, 1 - c, :, WB:WT], M["PA"] + u)
+    gbuf[:, WB:GU] = dot(xbuf[...], wbuf[:, :, :, :, WB:GU].reshape(D, 256), ((1,), (0,)))
     gate = gbuf[:, 0:FH]
-    hid[...] = (gate / (1.0 + jnp.exp(-gate)) * gbuf[:, FH:WB]).astype(BF16)
+    hid[...] = (gate / (1.0 + jnp.exp(-gate)) * gbuf[:, FH:GU]).astype(BF16)
 
     def feed(off):
-        return dot(hid[...], wbuf[pl.ds(at_y(off) * 2, 2), :, :, :, WB : WB + WA].reshape(DW, FH), ((1,), (1,)))
+        return dot(hid[...], wbuf[pl.ds(at_y(off) * 2, 2), :, :, :, GU:WT].reshape(DW, FH), ((1,), (1,)))
 
     for j in (2, 1, 3):
         fsend[j - 1] = feed(j).astype(BF16)
@@ -385,7 +436,7 @@
     for j in range(1, NY):
         arrived(frecv.at[j - 1], M["F"] + j)
     hres[...] += frecv[0].astype(F32) + frecv[1].astype(F32) + frecv[2].astype(F32)
-    out_ref[...] = norm(st2, sr2, M["S2"], g2_ref, b2_ref)
+    out_ref[...] = norm(st2, sr2, M["S2"], g2_ref, b2_ref, lambda: None)
 
     for j in range(1, NX):
         sent(qbuf.at[0, 0:96, :], M["Q"] + (j - 1) * 2)
@@ -400,19 +451,20 @@
         sent(fsend.at[0], M["F"] + j)
         sent(st2, M["S2"] + j)
     for d in range(1, 5):
-        for name, ref in (("K", kvbuf.at[0, 0]), ("A", a_row(0)), ("B", b_slot(0, 0))):
-            sent(ref, M[name + "M"] + d)
-            if d < 4:
-                sent(ref, M[name + "P"] + d)
+        for name, ref, last in (("K", kvbuf.at[0, 0], "M"), ("A", a_row(0), "P"), ("B", b_slot(0, 0), "M")):
+            for way in "MP":
+                if d < 4 or way == last:
+                    sent(ref, M[name + way] + d)
     for u in range(NZ):
         sent(kvbuf.at[0, 0], M["KT"] + u)
         sent(b_slot(0, 0), M["XP"] + u)
         sent(b_slot(0, 0), M["XM"] + u)
         sent(b_slot(0, 0), M["RL"] + u)
-        sent(wbuf.at[0, :, c], M["PW"] + u)
-    for i in (1, 2):
-        sent(x_part(0, every), M["G"] + i)
-        sent(x_part(0, first_half), M["G"] + 2 + i)
+        sent(a_row(0), M["PA"] + u)
+        for way in range(4):
+            sent(b_slot(0, 0), M["PB"] + 4 * u + way)
+    for j in range(1, NY):
+        sent(x_part(0), M["G"] + j)
 
 
 def body(
@@ -425,13 +477,12 @@
     freqs = THETA ** (-(2.0 * jnp.arange(quarter, dtype=F32)) / (2 * quarter))
     row_angle = freqs[:, None] * (positions // GRID_W).astype(F32)[None, :]
     col_angle = freqs[:, None] * (positions % GRID_W).astype(F32)[None, :]
-    tab = jnp.concatenate([jnp.cos(row_angle), jnp.sin(row_angle), jnp.cos(col_angle), jnp.sin(col_angle)], axis=0)
     row = lambda v: v.reshape(1, -1)
     operands = (
         residual, query_latent, shared_latent, rotary_key.T, row(query_gain), row(latent_gain), query_narrow.T,
-        key_narrow, value_narrow.T, query_wide.T, key_wide, value_wide.T, output_narrow, output_wide,
+        key_narrow.T, value_narrow.T, query_wide.T, key_wide, value_wide, output_narrow, output_wide,
         row(first_gain), row(first_bias), gate_weight, up_weight, down_weight.T, row(second_gain),
-        row(second_bias), tab,
+        row(second_bias), jnp.cos(row_angle), jnp.sin(row_angle), jnp.cos(col_angle), jnp.sin(col_angle),
     )
     vmem = pl.BlockSpec(memory_space=pltpu.VMEM)
     return pl.pallas_call(
@@ -442,7 +493,7 @@
         scratch_shapes=[
             pltpu.VMEM((NZ, 2, ROWS + ROPE, LAT), BF16),
             pltpu.VMEM((NX, KX, ROWS), BF16),
-            pltpu.VMEM((NZ, NX, 2, SLOT, WB + WA), BF16),
+            pltpu.VMEM((NZ, NX, 2, SLOT, WT), BF16),
             pltpu.VMEM((LAT, 256), BF16),
             pltpu.VMEM((VD, LAT), BF16),
             pltpu.VMEM((2 * ROWS, KX), BF16),
@@ -459,7 +510,7 @@
             pltpu.VMEM((8, ROWS), F32),
             pltpu.VMEM((3, 8, ROWS), F32),
             pltpu.VMEM((ROWS, D), BF16),
-            pltpu.VMEM((ROWS, WB), F32),
+            pltpu.VMEM((ROWS, GU), F32),
             pltpu.VMEM((ROWS, FH), BF16),
             pltpu.VMEM((3, ROWS, DW), BF16),
             pltpu.VMEM((3, ROWS, DW), BF16),

time: 128 us -> 102 us (0.80)
  Pallas kernels: 122 us -> 98.9 us
  local copies, waits for them, and re-layouts: 3.29 us -> 1.67 us
    pallas_call x1, Pallas kernels: 122 us -> 98.9 us  [body(): pl.pallas_call(layer_kernel, out_shape=jax.ShapeDtypeStruct((ROWS, DW), B...]
    unnamed x7 -> x1, local copies, waits for them, and re-layouts: 3.29 us -> 1.67 us
where the time goes in v2:
time: 102 us; the launch traced here: 101 us
  Pallas kernels  98.9 us (97%)
  local copies, waits for them, and re-layouts  1.67 us (2%)
    pallas_call x1, Pallas kernels, body(): pl.pallas_call(layer_kernel, out_shape=jax.ShapeDtypeStruct((ROWS, DW), B...  98.9 us

profile of v2, /device:TPU:1, one launch (start us, length us, event | category | flops | bytes accessed | tf_op | source)
XLA Modules:
  0.0 101.3 jit_solution(6767510623984122554)
XLA Ops:
  0.0 0.7 multiply_sine_fusion
  0.8 98.9 %shard_map.199 = bf16[256,512]{1,0:T(8,128)(2,1)} custom-call(bf16[256,512]{1,0:T(8,128)(2,1)} %res_ref.1, bf16[256,512]{1,0:T(8,128)(2,1)} %ql_ref.1, bf16[256,256]{1,0:T(8,128)(2,1)} %sl_ref.1, bf16[32,256]{1,0:T(8,128)(2,1)} %bitcast.17, f32[1,512]{1,0:T(1,128)} %bitcast.18, f32[1,256]{1,0:T(1,128)} %bitcast.23, bf16[96,512]{1,0:T(8,128)(2,1)} %bitcast.13, ...), custom_call_target="tpu_custom_call" | custom-call | tf_op jit(solution)/shard_map/pallas_call | solution.py:488
  99.7 1.7 %copy.23 = bf16[256,512]{1,0:T(8,128)(2,1)} copy(bf16[256,512]{1,0:T(8,128)(2,1)} %shard_map.199) | data formatting | bytes 524288
  (2 shorter events, 0.0 us)

commit v3 on v2

v3 whole, which is shorter than its diff:
```python
import jax
import jax.numpy as jnp
from jax import lax
from jax.experimental import pallas as pl
from jax.experimental.pallas import tpu as pltpu
from jax.sharding import PartitionSpec as P

ROPE = 32
NOPE_A = 64
V_A = 64
NOPE_B = 128
V_B = 128
GRID_W = 64
EPS_ROOT = 1e-06
EPS_LAYER = 1e-05
THETA = 10000.0
DEEP_ALPHA = 2.0**0.25
LOG2E = 1.4426950408889634

NZ, NX, NY = 8, 4, 4
ROWS = 256
HALF = ROWS // 2
LAT = 256
DW = 512
D = 2048
FH = 1408
GU = 2 * FH
WT = 3 * FH
WB = GU - 256
B_COLS, A_COLS = slice(0, WB), slice(WB, WT)
SLOT = 32
VD = V_A + V_B
KX = 128 + 256
C_A = (NOPE_A + ROPE) ** -0.5 * LOG2E
C_B = (NOPE_B + ROPE) ** -0.5 * LOG2E
MESH = pl.DeviceIdType.MESH
F32, BF16 = jnp.float32, jnp.bfloat16


def numbered(**counts):
    at, table = 0, {}
    for name, count in counts.items():
        table[name] = at
        at += count
    return table, at


M, MESSAGES = numbered(
    Q=6, KZ=8, KY=24, KT=8, O=4, OS=4, WO=6, AT=4, S1=4, G=6, F=6, S2=4,
    A1=4, AM=5, AP=5, BM=5, BP=4, XP=8, XM=8, RL=8, PB=32, PA=8,
)


def dot(a, b, dims):
    return lax.dot_general(a, b, (dims, ((), ())), preferred_element_type=F32)


def root_scale(latent, gain):
    x = latent.astype(F32)
    return x * lax.rsqrt(jnp.mean(x * x, axis=-1, keepdims=True) + EPS_ROOT) * gain


def turn(v, tab):
    cr, sr, cc, sc = tab
    a, b, c, d = v[0:8], v[8:16], v[16:24], v[24:32]
    return jnp.concatenate([a * cr - b * sr, b * cr + a * sr, c * cc - d * sc, d * cc + c * sc], axis=0)


def layer_kernel(
    res_hbm, ql_hbm, sl_hbm, rk_hbm, wqn_hbm, kn_hbm, vn_hbm, wqw_hbm, kw_hbm, vw_hbm, on_ref, ow_ref,
    gate_ref, up_ref, down_ref, qg_ref, lg_ref, g1_ref, b1_ref, g2_ref, b2_ref, cr_ref, sr_ref, cc_ref, sc_ref,
    out_ref,
    res_ref, ql_ref, sl_ref, rk_ref, wqn_ref, kn_ref, vn_ref, wqw_ref, kw_ref, vw_ref,
    kvbuf, qbuf, wbuf, wk, wv, kx, vx, ml, acc, osend, orecv, srecv, att, wo, st1, sr1, st2, sr2,
    xbuf, gbuf, hid, fsend, frecv, fthru, fkeep, hres, ss, rs, ls,
):
    s, t = lax.axis_index("sp"), lax.axis_index("tp")
    c = lax.rem(s, 2)
    x = lax.rem(lax.div(s, 2), NX)
    z = lax.div(s, 2 * NX)

    def at_z(off):
        return lax.rem(z + off + NZ, NZ)

    def at_x(off):
        return lax.rem(x + off + NX, NX)

    def at_y(off):
        return lax.rem(t + off + NY, NY)

    def dev_z(off):
        return (at_z(off) * (2 * NX) + x * 2 + c, t)

    def dev_x(off):
        return (z * (2 * NX) + at_x(off) * 2 + c, t)

    def dev_y(off):
        return (s, at_y(off))

    partner = (s + 1 - 2 * c, t)

    def zz(u):
        return at_z(lax.div(u + 1, 2) * (1 - 2 * lax.rem(u, 2)) if not isinstance(u, int) else (u + 1) // 2 * (1 - 2 * (u % 2)))


    def msg(src, dst, i, dev):
        return pltpu.make_async_remote_copy(
            src_ref=src, dst_ref=dst, send_sem=ss.at[i], recv_sem=rs.at[i],
            device_id=dev, device_id_type=MESH,
        )

    def send(src, dst, i, dev):
        msg(src, dst, i, dev).start()

    def arrived(dst, i):
        msg(dst, dst, i, partner).wait_recv()

    def sent(src, i):
        msg(src, src, i, partner).wait_send()

    b_slot = lambda zi, xi: wbuf.at[zi, xi, c, :, B_COLS]
    a_slot = lambda zi, xi: wbuf.at[zi, xi, c, :, A_COLS]
    a_row = lambda zi: wbuf.at[zi, :, c, :, A_COLS]

    barrier = pltpu.get_barrier_semaphore()
    friends = [*[dev_z(off) for off in range(1, NZ)], dev_x(1), dev_x(2), dev_x(3), partner, dev_y(1), dev_y(2), dev_y(3)]
    for f in friends:
        pl.semaphore_signal(barrier, inc=1, device_id=f, device_id_type=MESH)

    my_cols = pl.ds(pl.multiple_of(t * DW, DW), DW)
    local = [
        (sl_hbm, sl_ref), (rk_hbm, rk_ref), (ql_hbm, ql_ref), (wqn_hbm, wqn_ref), (wqw_hbm, wqw_ref),
        (kn_hbm, kn_ref), (kw_hbm, kw_ref), (vn_hbm, vn_ref), (vw_hbm, vw_ref),
        (gate_ref, wbuf.at[z, x, c, :, 0:FH]), (up_ref, wbuf.at[z, x, c, :, FH:GU]),
        (down_ref, wbuf.at[z, x, c, :, GU:WT]), (on_ref.at[:, my_cols], wo.at[t, 0:V_A, :]),
        (ow_ref.at[:, my_cols], wo.at[t, V_A:VD, :]), (res_hbm, res_ref),
    ]
    local = [pltpu.make_async_copy(src, dst, ls.at[i]) for i, (src, dst) in enumerate(local)]
    for o in local:
        o.start()
    for o in local[:9]:
        o.wait()

    tab = (cr_ref[...], sr_ref[...], cc_ref[...], sc_ref[...])
    latent = root_scale(sl_ref[...], lg_ref[...]).astype(BF16)
    turned = turn(rk_ref[...].astype(F32), tab)
    for q in range(NY):
        kvbuf[z, c, q, 0:64, :] = latent[q * 64 : (q + 1) * 64]
        kvbuf[z, c, q, 64:80, :] = jnp.concatenate([turned[q * 8 : (q + 1) * 8], jnp.zeros((8, ROWS), F32)], axis=0).astype(BF16)
    qn = root_scale(ql_ref[...], qg_ref[...]).astype(BF16)
    narrow = dot(wqn_ref[...], qn, ((1,), (1,)))
    wide = dot(wqw_ref[...], qn, ((1,), (1,)))
    qbuf[x, 0:96, :] = jnp.concatenate([narrow[0:NOPE_A], turn(narrow[NOPE_A:], tab)], axis=0).astype(BF16)
    qbuf[x, 224:384, :] = jnp.concatenate([turn(wide[NOPE_B:], tab), wide[0:NOPE_B]], axis=0).astype(BF16)
    for j in range(NX):
        qbuf[j, 96:224, :] = jnp.zeros((128, ROWS), BF16)
    wk[:, 0:64] = kn_ref[...].T
    wk[:, 64:128] = jnp.zeros((LAT, 64), BF16)
    wk[:, 128:256] = kw_ref[...]
    wv[0:V_A, :] = vn_ref[...]
    wv[V_A:VD, :] = vw_ref[...].T

    pl.semaphore_wait(barrier, len(friends))

    for off in (1, 7, 2, 6, 3, 5, 4):
        send(kvbuf.at[z, c, t], kvbuf.at[z, c, t], M["KZ"] + off, dev_z(off))
    send(kvbuf.at[z, c], kvbuf.at[z, c], M["KT"], partner)
    for j in (2, 1, 3):
        for half, rows in enumerate((slice(0, 96), slice(224, 384))):
            send(qbuf.at[x, rows, :], qbuf.at[x, rows, :], M["Q"] + (j - 1) * 2 + half, dev_x(j))
    for o in local[9:12]:
        o.wait()

    def to_partner(u, zi, way):
        xi = at_x((0, -1, 1, 2)[way])
        send(b_slot(zi, xi), b_slot(zi, xi), M["PB"] + 4 * u + way, partner)

    def row_to_partner(u, zi):
        send(a_row(zi), a_row(zi), M["PA"] + u, partner)

    def to_x(u, zi):
        send(b_slot(zi, x), b_slot(zi, x), M["XP"] + u, dev_x(1))
        send(b_slot(zi, x), b_slot(zi, x), M["XM"] + u, dev_x(-1))

    def start_a():
        for j in (2, 1, 3):
            send(a_slot(z, x), a_slot(z, x), M["A1"] + j, dev_x(j))

    def start_b():
        send(b_slot(z, x), b_slot(z, x), M["BM"] + 1, dev_z(-1))
        send(b_slot(z, x), b_slot(z, x), M["BP"] + 1, dev_z(1))
        to_x(0, z)
        to_partner(0, z, 0)

    def start_rows():
        for j in range(1, NX):
            arrived(a_slot(z, at_x(-j)), M["A1"] + j)
        send(a_row(z), a_row(z), M["AM"] + 1, dev_z(-1))
        send(a_row(z), a_row(z), M["AP"] + 1, dev_z(1))
        row_to_partner(0, z)

    def rows_round(d):
        below, above = at_z(-d), at_z(d)
        cut = (lambda ref, half: ref) if d < 3 else lambda ref, half: ref.at[slice(2 * half, 2 * half + 2)]
        if d == 4:
            arrived(cut(a_row(below), 0), M["AP"] + d)
            arrived(cut(a_row(below), 1), M["AM"] + d)
            row_to_partner(7, below)
            return
        arrived(a_row(below), M["AP"] + d)
        send(cut(a_row(below), 0), cut(a_row(below), 0), M["AP"] + d + 1, dev_z(1))
        row_to_partner(2 * d - 1, below)
        arrived(a_row(above), M["AM"] + d)
        send(cut(a_row(above), 1), cut(a_row(above), 1), M["AM"] + d + 1, dev_z(-1))
        row_to_partner(2 * d, above)

    def slots_round(d, sideways=True):
        up, low = 2 * d - d // 4, 2 * d - 1
        arrived(b_slot(at_z(d), x), M["BM"] + d)
        if d < 4:
            send(b_slot(at_z(d), x), b_slot(at_z(d), x), M["BM"] + d + 1, dev_z(-1))
        to_partner(up, at_z(d), 0)
        if sideways:
            to_x(up, at_z(d))
        if d < 4:
            arrived(b_slot(at_z(-d), x), M["BP"] + d)
            if d < 3:
                send(b_slot(at_z(-d), x), b_slot(at_z(-d), x), M["BP"] + d + 1, dev_z(1))
            to_partner(low, at_z(-d), 0)
            if sideways:
                to_x(low, at_z(-d))

    plus = (0, 1, 3, 5)

    def relay(u):
        zu = zz(u)
        arrived(b_slot(zu, at_x(-1)), M["XP"] + u)
        if u in plus:
            send(b_slot(zu, at_x(-1)), b_slot(zu, at_x(-1)), M["RL"] + u, dev_x(1))
        to_partner(u, zu, 1)
        arrived(b_slot(zu, at_x(1)), M["XM"] + u)
        if u not in plus:
            send(b_slot(zu, at_x(1)), b_slot(zu, at_x(1)), M["RL"] + u, dev_x(-1))
        to_partner(u, zu, 2)

    def across(u):
        arrived(b_slot(zz(u), at_x(2)), M["RL"] + u)
        to_partner(u, zz(u), 3)

    def partner_block(u):
        for way in range(4):
            arrived(wbuf.at[zz(u), at_x((0, -1, 1, 2)[way]), 1 - c, :, B_COLS], M["PB"] + 4 * u + way)

    start_a()
    start_b()
    def send_wo():
        for j in (2, 1, 3):
            cols = pl.ds(pl.multiple_of(at_y(j) * DW, DW), DW)
            send(on_ref.at[:, cols], wo.at[t, 0:V_A, :], M["WO"] + (j - 1) * 2, dev_y(j))
            send(ow_ref.at[:, cols], wo.at[t, V_A:VD, :], M["WO"] + (j - 1) * 2 + 1, dev_y(j))

    for j in range(NX):
        ml[j] = jnp.concatenate([jnp.full((2, ROWS), -jnp.inf, F32), jnp.zeros((6, ROWS), F32)], axis=0)
        acc[j] = jnp.zeros((VD, ROWS), F32)

    def keys_of(zs):
        lane = lax.broadcasted_iota(jnp.int32, (ROWS, 128), 1)
        for core in range(2):
            latent = kvbuf[zs, core, :, 0:64, :].reshape(ROWS, LAT)
            turned = jnp.concatenate([kvbuf[zs, core, q, 64:80, :].astype(F32)[0:8] for q in range(NY)], axis=0)
            rot = jnp.concatenate([jnp.zeros((64, ROWS), F32), turned, turned], axis=0).T
            keys = dot(latent, wk[...], ((1,), (0,)))
            at = slice(core * ROWS, (core + 1) * ROWS)
            kx[at, 0:128] = jnp.where(lane < 64, keys[:, 0:128], rot).astype(BF16)
            kx[at, 128:256] = rot.astype(BF16)
            kx[at, 256:384] = keys[:, 128:256].astype(BF16)
            vx[:, at] = dot(wv[...], latent, ((1,), (1,))).astype(BF16)

    def attend(zs):
        keys_of(zs)

        heads = ((0, 128, 0, V_A, C_A), (128, 384, V_A, VD, C_B))
        every_score = [
            [dot(kx[:, lo:hi], qbuf[j, lo:hi, :], ((1,), (0,))) for lo, hi, _, _, _ in heads] for j in range(NX)
        ]
        for j in range(NX):
            for h, (_, _, vlo, vhi, scale) in enumerate(heads):
                scores = every_score[j][h]
                old = ml[j, h : h + 1, :]
                new = jnp.maximum(old, jnp.max(scores, axis=0, keepdims=True))
                factor = jnp.exp2((old - new) * scale)
                raised = jnp.exp2((scores - new) * scale)
                ml[j, h : h + 1, :] = new
                ml[j, 2 + h : 3 + h, :] = ml[j, 2 + h : 3 + h, :] * factor + jnp.sum(raised, axis=0, keepdims=True)
                acc[j, vlo:vhi, :] = acc[j, vlo:vhi, :] * factor + dot(vx[vlo:vhi, :], raised.astype(BF16), ((1,), (0,)))

    def quarter_out(u):
        d = (u + 1) // 2
        slot = kvbuf.at[zz(u), c, t]
        arrived(slot, M["KZ"] + (d if u % 2 else NZ - d))
        for j in (2, 1, 3):
            send(slot, slot, M["KY"] + 3 * u + j - 1, dev_y(j))

    def latents_across(u):
        zu = zz(u)
        for j in range(1, NY):
            arrived(kvbuf.at[zu, c, at_y(-j)], M["KY"] + 3 * u + j - 1)
        send(kvbuf.at[zu, c], kvbuf.at[zu, c], M["KT"] + u, partner)

    def on_step(k, value, then):
        @pl.when(k == value)
        def _():
            then()

    def unit(i, carry):
        @pl.when(i == 0)
        def _():
            quarter_out(1)
            quarter_out(2)
            for j in range(1, NX):
                for half, rows in enumerate((slice(0, 96), slice(224, 384))):
                    arrived(qbuf.at[at_x(-j), rows, :], M["Q"] + (j - 1) * 2 + half)
            quarter_out(3)
            quarter_out(4)

        on_step(i, 1, lambda: (quarter_out(5), quarter_out(6), quarter_out(7), send_wo(), slots_round(1)))
        on_step(i, 2, lambda: start_rows())
        on_step(i, 4, lambda: slots_round(2))

        @pl.when(i < 7)
        def _():
            latents_across(i + 1)

        zi = zz(i)
        arrived(kvbuf.at[zi, 1 - c], M["KT"] + i)
        attend(zi)
        return carry

    lax.fori_loop(0, NZ, unit, 0)

    for j in range(NX):
        for h, (vlo, vhi) in enumerate(((0, V_A), (V_A, VD))):
            osend[j, vlo:vhi, :] = (acc[j, vlo:vhi, :] / ml[j, 2 + h : 3 + h, :]).astype(BF16)
    for j in (2, 1, 3):
        send(osend.at[at_x(j)], orecv.at[j - 1], M["O"] + j, dev_x(j))
        send(ml.at[at_x(j)], srecv.at[j - 1], M["OS"] + j, dev_x(j))

    rows_round(1)
    slots_round(3)
    relay(0)
    for j in range(1, NX):
        arrived(orecv.at[j - 1], M["O"] + j)
        arrived(srecv.at[j - 1], M["OS"] + j)
    for h, (vlo, vhi, scale) in enumerate(((0, V_A, C_A), (V_A, VD, C_B))):
        tops = [ml[x, h : h + 1, :]] + [srecv[j, h : h + 1, :] for j in range(3)]
        sums = [ml[x, 2 + h : 3 + h, :]] + [srecv[j, 2 + h : 3 + h, :] for j in range(3)]
        parts = [osend[x, vlo:vhi, :]] + [orecv[j, vlo:vhi, :] for j in range(3)]
        top = jnp.maximum(jnp.maximum(tops[0], tops[1]), jnp.maximum(tops[2], tops[3]))
        shares = [total * jnp.exp2((m - top) * scale) for m, total in zip(tops, sums)]
        total = shares[0] + shares[1] + shares[2] + shares[3]
        mixed = sum(part.astype(F32) * (share / total) for part, share in zip(parts, shares))
        att[t, vlo:vhi, :] = mixed.astype(BF16)
    for j in (2, 1, 3):
        send(att.at[t], att.at[t], M["AT"] + j, dev_y(j))

    relay(1)
    relay(2)

    for o in local[12:]:
        o.wait()
    for j in range(1, NY):
        for half, rows in enumerate((slice(0, V_A), slice(V_A, VD))):
            arrived(wo.at[at_y(-j), rows, :], M["WO"] + (j - 1) * 2 + half)
    for j in range(1, NY):
        arrived(att.at[at_y(-j)], M["AT"] + j)

    def norm(stat, got, first, gain_ref, bias_ref, between):
        h = hres[...]
        center = jnp.mean(h, axis=1, keepdims=True)
        apart = jnp.sum((h - center) * (h - center), axis=1, keepdims=True)
        lane = lax.broadcasted_iota(jnp.int32, (ROWS, 128), 1)
        both = jnp.where(lane == 0, center, jnp.where(lane == 1, apart, 0.0))
        stat[...] = both.T[0:8]
        for j in (2, 1, 3):
            send(stat, got.at[j - 1], first + j, dev_y(j))
        between()
        for j in range(1, NY):
            arrived(got.at[j - 1], first + j)
        centers = [stat[0:1, :]] + [got[j, 0:1, :] for j in range(3)]
        aparts = [stat[1:2, :]] + [got[j, 1:2, :] for j in range(3)]
        middle = (centers[0] + centers[1] + centers[2] + centers[3]) * 0.25
        spread = sum(aparts) + DW * sum((m - middle) * (m - middle) for m in centers)
        root = lax.rsqrt(spread * (1.0 / D) + EPS_LAYER)
        cols = jnp.concatenate([middle, root, jnp.zeros((126, ROWS), F32)], axis=0).T
        return ((h - cols[:, 0:1]) * cols[:, 1:2] * gain_ref[...] + bias_ref[...]).astype(BF16)

    mixed = dot(att[...].reshape(NY * VD, ROWS), wo[...].reshape(NY * VD, DW), ((0,), (0,)))
    hres[...] = DEEP_ALPHA * res_ref[...].astype(F32) + mixed
    normed = norm(st1, sr1, M["S1"], g1_ref, b1_ref, lambda: (slots_round(4), relay(3)))
    xbuf[:, my_cols] = normed
    hres[...] = DEEP_ALPHA * normed.astype(F32)

    def x_half(off, half):
        return xbuf.at[pl.ds(half * HALF, HALF), pl.ds(pl.multiple_of(at_y(off) * DW, DW), DW)]

    def send_x(off, half, i, way):
        send(x_half(off, half), x_half(off, half), M["G"] + i, dev_y(way))

    for i, half, way in ((0, 0, 1), (2, 1, -1), (1, 1, 1), (3, 0, -1)):
        send_x(0, half, i, way)
    rows_round(2)
    relay(4)
    across(0)
    across(1)
    arrived(x_half(-1, 0), M["G"])
    send_x(-1, 0, 4, 1)
    arrived(x_half(1, 1), M["G"] + 2)
    send_x(1, 1, 5, -1)
    rows_round(3)
    relay(5)
    across(2)
    relay(6)
    across(3)
    relay(7)
    for i, off, half in ((1, -1, 1), (3, 1, 0), (4, 2, 0), (5, 2, 1)):
        arrived(x_half(off, half), M["G"] + i)

    def gate_up(u):
        zu = zz(u)
        features = xbuf[:, pl.ds(pl.multiple_of(zu * 256, 256), 256)]
        for n in range(WB // 256):
            cols = slice(n * 256, (n + 1) * 256)
            part = dot(features, wbuf[zu, :, :, :, cols].reshape(256, 256), ((1,), (0,)))
            gbuf[:, cols] = part if isinstance(u, int) else gbuf[:, cols] + part

    partner_block(0)
    gate_up(0)

    def block(u, carry):
        @pl.when(u <= 4)
        def _():
            across(u + 3)

        partner_block(u)
        gate_up(u)
        return carry

    lax.fori_loop(1, NZ, block, 0)
    rows_round(4)
    for u in range(NZ):
        arrived(wbuf.at[zz(u), :, 1 - c, :, A_COLS], M["PA"] + u)
    gbuf[:, WB:GU] = dot(xbuf[...], wbuf[:, :, :, :, WB:GU].reshape(D, 256), ((1,), (0,)))
    gate = gbuf[:, 0:FH]
    hid[...] = (gate / (1.0 + jnp.exp(-gate)) * gbuf[:, FH:GU]).astype(BF16)

    def feed(off):
        return dot(hid[...], wbuf[pl.ds(at_y(off) * 2, 2), :, :, :, GU:WT].reshape(DW, FH), ((1,), (1,)))

    first, second = slice(0, HALF), slice(HALF, ROWS)
    fsend[1] = feed(2).astype(BF16)
    send(fsend.at[1, first], fthru.at[0], M["F"], dev_y(1))
    send(fsend.at[1, second], fthru.at[1], M["F"] + 1, dev_y(-1))
    after = feed(1)
    fsend[0, second] = after[second].astype(BF16)
    send(fsend.at[0, second], frecv.at[0, second], M["F"] + 2, dev_y(1))
    fkeep[0] = after[first]
    before = feed(3)
    fsend[2, first] = before[first].astype(BF16)
    send(fsend.at[2, first], frecv.at[1, first], M["F"] + 3, dev_y(-1))
    fkeep[1] = before[second]
    arrived(fthru.at[0], M["F"])
    fsend[0, first] = (fkeep[0] + fthru[0].astype(F32)).astype(BF16)
    send(fsend.at[0, first], frecv.at[0, first], M["F"] + 4, dev_y(1))
    arrived(fthru.at[1], M["F"] + 1)
    fsend[2, second] = (fkeep[1] + fthru[1].astype(F32)).astype(BF16)
    send(fsend.at[2, second], frecv.at[1, second], M["F"] + 5, dev_y(-1))
    hres[...] += feed(0)
    for i, k, rows in ((2, 0, second), (3, 1, first), (4, 0, first), (5, 1, second)):
        arrived(frecv.at[k, rows], M["F"] + i)
    hres[...] += frecv[0].astype(F32) + frecv[1].astype(F32)
    out_ref[...] = norm(st2, sr2, M["S2"], g2_ref, b2_ref, lambda: None)

    for j in range(1, NX):
        sent(qbuf.at[0, 0:96, :], M["Q"] + (j - 1) * 2)
        sent(qbuf.at[0, 224:384, :], M["Q"] + (j - 1) * 2 + 1)
        sent(a_slot(0, 0), M["A1"] + j)
        sent(osend.at[0], M["O"] + j)
        sent(ml.at[0], M["OS"] + j)
        sent(wo.at[0, 0:V_A, :], M["WO"] + (j - 1) * 2)
        sent(wo.at[0, V_A:VD, :], M["WO"] + (j - 1) * 2 + 1)
        sent(att.at[0], M["AT"] + j)
        sent(st1, M["S1"] + j)
        sent(st2, M["S2"] + j)
    for d in range(1, 5):
        for way in "MP":
            sent(a_row(0) if d < 4 else a_row(0).at[0:2], M["A" + way] + d)
            if d < 4 or way == "M":
                sent(b_slot(0, 0), M["B" + way] + d)
    for u in range(NZ):
        sent(kvbuf.at[0, 0], M["KT"] + u)
        if u > 0:
            sent(kvbuf.at[0, 0, 0], M["KZ"] + u)
            for j in range(1, NY):
                sent(kvbuf.at[0, 0, 0], M["KY"] + 3 * u + j - 1)
        sent(a_row(0), M["PA"] + u)
        for way in range(4):
            sent(b_slot(0, 0), M["PB"] + 4 * u + way)
        for name in ("XP", "XM", "RL"):
            sent(b_slot(0, 0), M[name] + u)
    for i in range(6):
        sent(x_half(0, 0), M["G"] + i)
        sent(fsend.at[0, 0:HALF], M["F"] + i)


def body(
    residual, query_latent, shared_latent, rotary_key, query_gain, latent_gain, query_narrow, key_narrow,
    value_narrow, query_wide, key_wide, value_wide, output_narrow, output_wide, first_gain, first_bias,
    gate_weight, up_weight, down_weight, second_gain, second_bias,
):
    positions = lax.axis_index("sp") * ROWS + jnp.arange(ROWS, dtype=jnp.int32)
    quarter = ROPE // 4
    freqs = THETA ** (-(2.0 * jnp.arange(quarter, dtype=F32)) / (2 * quarter))
    row_angle = freqs[:, None] * (positions // GRID_W).astype(F32)[None, :]
    col_angle = freqs[:, None] * (positions % GRID_W).astype(F32)[None, :]
    row = lambda v: v.reshape(1, -1)
    large = (
        residual, query_latent, shared_latent, rotary_key.T, query_narrow.T, key_narrow.T, value_narrow.T,
        query_wide.T, key_wide, value_wide, output_narrow, output_wide, gate_weight, up_weight, down_weight.T,
    )
    small = (
        row(query_gain), row(latent_gain), row(first_gain), row(first_bias), row(second_gain), row(second_bias),
        jnp.cos(row_angle), jnp.sin(row_angle), jnp.cos(col_angle), jnp.sin(col_angle),
    )
    vmem = pl.BlockSpec(memory_space=pltpu.VMEM)
    return pl.pallas_call(
        layer_kernel,
        out_shape=jax.ShapeDtypeStruct((ROWS, DW), BF16),
        in_specs=[pl.BlockSpec(memory_space=pl.ANY)] * len(large) + [vmem] * len(small),
        out_specs=vmem,
        scratch_shapes=[
            *[pltpu.VMEM(v.shape, v.dtype) for v in large[:10]],
            pltpu.VMEM((NZ, 2, NY, 80, LAT), BF16),
            pltpu.VMEM((NX, KX, ROWS), BF16),
            pltpu.VMEM((NZ, NX, 2, SLOT, WT), BF16),
            pltpu.VMEM((LAT, 256), BF16),
            pltpu.VMEM((VD, LAT), BF16),
            pltpu.VMEM((2 * ROWS, KX), BF16),
            pltpu.VMEM((VD, 2 * ROWS), BF16),
            pltpu.VMEM((NX, 8, ROWS), F32),
            pltpu.VMEM((NX, VD, ROWS), F32),
            pltpu.VMEM((NX, VD, ROWS), BF16),
            pltpu.VMEM((3, VD, ROWS), BF16),
            pltpu.VMEM((3, 8, ROWS), F32),
            pltpu.VMEM((NY, VD, ROWS), BF16),
            pltpu.VMEM((NY, VD, DW), BF16),
            pltpu.VMEM((8, ROWS), F32),
            pltpu.VMEM((3, 8, ROWS), F32),
            pltpu.VMEM((8, ROWS), F32),
            pltpu.VMEM((3, 8, ROWS), F32),
            pltpu.VMEM((ROWS, D), BF16),
            pltpu.VMEM((ROWS, GU), F32),
            pltpu.VMEM((ROWS, FH), BF16),
            pltpu.VMEM((3, ROWS, DW), BF16),
            pltpu.VMEM((2, ROWS, DW), BF16),
            pltpu.VMEM((2, HALF, DW), BF16),
            pltpu.VMEM((2, HALF, DW), F32),
            pltpu.VMEM((ROWS, DW), F32),
            pltpu.SemaphoreType.DMA((MESSAGES,)),
            pltpu.SemaphoreType.DMA((MESSAGES,)),
            pltpu.SemaphoreType.DMA((len(large),)),
        ],
        compiler_params=pltpu.CompilerParams(
            collective_id=0, has_side_effects=True, vmem_limit_bytes=60 * 1024 * 1024
        ),
    )(*large, *small)


def solution(mesh):
    return jax.shard_map(
        body,
        mesh=mesh,
        in_specs=(
            P("sp", "tp"),
            P("sp", None),
            P("sp", None),
            P("sp", None),
            P(),
            P(),
            P(None, "tp"),
            P(None, "tp"),
            P(None, "tp"),
            P(None, "tp"),
            P(None, "tp"),
            P(None, "tp"),
            P("tp", None),
            P("tp", None),
            P("tp"),
            P("tp"),
            P("sp", "tp"),
            P("sp", "tp"),
            P("tp", "sp"),
            P("tp"),
            P("tp"),
        ),
        out_specs=P("sp", "tp"),
        check_vma=False,
    )
```

time: 102 us -> 99.6 us (0.976)
  Pallas kernels: 98.9 us -> 95.8 us
    pallas_call x1, Pallas kernels: 98.9 us -> 95.8 us  [body(): pl.pallas_call(layer_kernel, out_shape=jax.ShapeDtypeStruct((ROWS, DW), B...]
where the time goes in v3:
time: 99.6 us; the launch traced here: 98.2 us
  Pallas kernels  95.8 us (96%)
  local copies, waits for them, and re-layouts  1.67 us (2%)
    pallas_call x1, Pallas kernels, body(): pl.pallas_call(layer_kernel, out_shape=jax.ShapeDtypeStruct((ROWS, DW), B...  95.8 us

profile of v3, /device:TPU:1, one launch (start us, length us, event | category | flops | bytes accessed | tf_op | source)
XLA Modules:
  0.0 98.2 jit_solution(14641567266690636052)
XLA Ops:
  0.0 0.7 multiply_sine_fusion
  0.8 95.8 %shard_map.199 = bf16[256,512]{1,0:T(8,128)(2,1)} custom-call(bf16[256,512]{1,0:T(8,128)(2,1)} %res_hbm.1, bf16[256,512]{1,0:T(8,128)(2,1)} %ql_hbm.1, bf16[256,256]{1,0:T(8,128)(2,1)} %sl_hbm.1, bf16[32,256]{1,0:T(8,128)(2,1)} %bitcast.17, bf16[96,512]{1,0:T(8,128)(2,1)} %bitcast.13, bf16[64,256]{1,0:T(8,128)(2,1)} %bitcast.15, bf16[64,256]{1,0:T(8,128)(2,1)} %bitcast.16, ...), custom_call_target="tpu_custom_call" | custom-call | tf_op jit(solution)/shard_map/pallas_call | solution.py:535
  96.5 1.7 %copy.23 = bf16[256,512]{1,0:T(8,128)(2,1)} copy(bf16[256,512]{1,0:T(8,128)(2,1)} %shard_map.199) | data formatting | bytes 524288
  (2 shorter events, 0.0 us)

commit v4 on v3

--- a/solution.py
+++ b/solution.py
@@ -20,13 +20,14 @@
 NZ, NX, NY = 8, 4, 4
 ROWS = 256
 HALF = ROWS // 2
+QUART = ROWS // 4
 LAT = 256
 DW = 512
 D = 2048
 FH = 1408
 GU = 2 * FH
 WT = 3 * FH
-WB = GU - 256
+WB = GU - 512
 B_COLS, A_COLS = slice(0, WB), slice(WB, WT)
 SLOT = 32
 VD = V_A + V_B
@@ -46,8 +47,8 @@
 
 
 M, MESSAGES = numbered(
-    Q=6, KZ=8, KY=24, KT=8, O=4, OS=4, WO=6, AT=4, S1=4, G=6, F=6, S2=4,
-    A1=4, AM=5, AP=5, BM=5, BP=4, XP=8, XM=8, RL=8, PB=32, PA=8,
+    Q=6, KZ=8, KY=24, KT=8, O=4, OS=4, WO=6, WP=4, RS=4, GN=8, AT=4, G=6, F=6, S2=4,
+    A1=4, AM=20, AP=20, BM=5, BP=4, XP=8, XM=8, RL=8, PB=32, PA=8,
 )
 
 
@@ -70,8 +71,8 @@
     res_hbm, ql_hbm, sl_hbm, rk_hbm, wqn_hbm, kn_hbm, vn_hbm, wqw_hbm, kw_hbm, vw_hbm, on_ref, ow_ref,
     gate_ref, up_ref, down_ref, qg_ref, lg_ref, g1_ref, b1_ref, g2_ref, b2_ref, cr_ref, sr_ref, cc_ref, sc_ref,
     out_ref,
-    res_ref, ql_ref, sl_ref, rk_ref, wqn_ref, kn_ref, vn_ref, wqw_ref, kw_ref, vw_ref,
-    kvbuf, qbuf, wbuf, wk, wv, kx, vx, ml, acc, osend, orecv, srecv, att, wo, st1, sr1, st2, sr2,
+    ql_ref, sl_ref, rk_ref, wqn_ref, kn_ref, vn_ref, wqw_ref, kw_ref, vw_ref,
+    kvbuf, qbuf, wbuf, wk, wv, kx, vx, ml, acc, osend, orecv, srecv, attended, attsend, att, wo, resq, gfull, st2, sr2,
     xbuf, gbuf, hid, fsend, frecv, fthru, fkeep, hres, ss, rs, ls,
 ):
     s, t = lax.axis_index("sp"), lax.axis_index("tp")
@@ -132,8 +133,9 @@
         (sl_hbm, sl_ref), (rk_hbm, rk_ref), (ql_hbm, ql_ref), (wqn_hbm, wqn_ref), (wqw_hbm, wqw_ref),
         (kn_hbm, kn_ref), (kw_hbm, kw_ref), (vn_hbm, vn_ref), (vw_hbm, vw_ref),
         (gate_ref, wbuf.at[z, x, c, :, 0:FH]), (up_ref, wbuf.at[z, x, c, :, FH:GU]),
-        (down_ref, wbuf.at[z, x, c, :, GU:WT]), (on_ref.at[:, my_cols], wo.at[t, 0:V_A, :]),
-        (ow_ref.at[:, my_cols], wo.at[t, V_A:VD, :]), (res_hbm, res_ref),
+        (down_ref, wbuf.at[z, x, c, :, GU:WT]), (on_ref, wo.at[t, 0:V_A, :]), (ow_ref, wo.at[t, V_A:VD, :]),
+        (res_hbm.at[pl.ds(pl.multiple_of(t * QUART, QUART), QUART), :], resq.at[:, my_cols]),
+        (g1_ref, gfull.at[0, :, my_cols]), (b1_ref, gfull.at[1, :, my_cols]),
     ]
     local = [pltpu.make_async_copy(src, dst, ls.at[i]) for i, (src, dst) in enumerate(local)]
     for o in local:
@@ -182,37 +184,42 @@
         send(b_slot(zi, x), b_slot(zi, x), M["XP"] + u, dev_x(1))
         send(b_slot(zi, x), b_slot(zi, x), M["XM"] + u, dev_x(-1))
 
+    def send_rows(zi, d, r):
+        slot = a_slot(zi, at_x(-r))
+        send(slot, slot, M["AP"] + 4 * d + r, dev_z(1))
+        send(slot, slot, M["AM"] + 4 * d + r, dev_z(-1))
+
     def start_a():
+        send_rows(z, 1, 0)
         for j in (2, 1, 3):
             send(a_slot(z, x), a_slot(z, x), M["A1"] + j, dev_x(j))
 
     def start_b():
         send(b_slot(z, x), b_slot(z, x), M["BM"] + 1, dev_z(-1))
         send(b_slot(z, x), b_slot(z, x), M["BP"] + 1, dev_z(1))
-        to_x(0, z)
         to_partner(0, z, 0)
 
     def start_rows():
-        for j in range(1, NX):
-            arrived(a_slot(z, at_x(-j)), M["A1"] + j)
-        send(a_row(z), a_row(z), M["AM"] + 1, dev_z(-1))
-        send(a_row(z), a_row(z), M["AP"] + 1, dev_z(1))
+        for r in (1, 3, 2):
+            arrived(a_slot(z, at_x(-r)), M["A1"] + r)
+            send_rows(z, 1, r)
         row_to_partner(0, z)
 
-    def rows_round(d):
+    def rows_round(d, *rs):
         below, above = at_z(-d), at_z(d)
-        cut = (lambda ref, half: ref) if d < 3 else lambda ref, half: ref.at[slice(2 * half, 2 * half + 2)]
-        if d == 4:
-            arrived(cut(a_row(below), 0), M["AP"] + d)
-            arrived(cut(a_row(below), 1), M["AM"] + d)
-            row_to_partner(7, below)
-            return
-        arrived(a_row(below), M["AP"] + d)
-        send(cut(a_row(below), 0), cut(a_row(below), 0), M["AP"] + d + 1, dev_z(1))
-        row_to_partner(2 * d - 1, below)
-        arrived(a_row(above), M["AM"] + d)
-        send(cut(a_row(above), 1), cut(a_row(above), 1), M["AM"] + d + 1, dev_z(-1))
-        row_to_partner(2 * d, above)
+        for r in rs:
+            if d < 4 or r < 2:
+                arrived(a_slot(below, at_x(-r)), M["AP"] + 4 * d + r)
+            if d < 3 or d == 3 and r < 2:
+                send(a_slot(below, at_x(-r)), a_slot(below, at_x(-r)), M["AP"] + 4 * d + 4 + r, dev_z(1))
+            if d < 4 or r >= 2:
+                arrived(a_slot(above, at_x(-r)), M["AM"] + 4 * d + r)
+            if d < 3 or d == 3 and r >= 2:
+                send(a_slot(above, at_x(-r)), a_slot(above, at_x(-r)), M["AM"] + 4 * d + 4 + r, dev_z(-1))
+            if r == 2:
+                row_to_partner(2 * d - 1, below)
+                if d < 4:
+                    row_to_partner(2 * d, above)
 
     def slots_round(d, sideways=True):
         up, low = 2 * d - d // 4, 2 * d - 1
@@ -251,13 +258,26 @@
         for way in range(4):
             arrived(wbuf.at[zz(u), at_x((0, -1, 1, 2)[way]), 1 - c, :, B_COLS], M["PB"] + 4 * u + way)
 
+    start_b()
     start_a()
-    start_b()
+    to_x(0, z)
+    wo_half = lambda core: pl.ds(pl.multiple_of(core * (D // 2), D // 2), D // 2)
+
     def send_wo():
         for j in (2, 1, 3):
-            cols = pl.ds(pl.multiple_of(at_y(j) * DW, DW), DW)
-            send(on_ref.at[:, cols], wo.at[t, 0:V_A, :], M["WO"] + (j - 1) * 2, dev_y(j))
-            send(ow_ref.at[:, cols], wo.at[t, V_A:VD, :], M["WO"] + (j - 1) * 2 + 1, dev_y(j))
+            rows = pl.ds(pl.multiple_of(at_y(j) * QUART, QUART), QUART)
+            send(res_hbm.at[rows, :], resq.at[:, my_cols], M["RS"] + j, dev_y(j))
+            send(g1_ref, gfull.at[0, :, my_cols], M["GN"] + j, dev_y(j))
+            send(b1_ref, gfull.at[1, :, my_cols], M["GN"] + 4 + j, dev_y(j))
+        for j in (2, 1, 3):
+            send(on_ref.at[:, wo_half(c)], wo.at[t, 0:V_A, wo_half(c)], M["WO"] + (j - 1) * 2, dev_y(j))
+            send(ow_ref.at[:, wo_half(c)], wo.at[t, V_A:VD, wo_half(c)], M["WO"] + (j - 1) * 2 + 1, dev_y(j))
+
+    def wo_across():
+        for j in range(1, NY):
+            arrived(wo.at[at_y(-j), 0:V_A, wo_half(c)], M["WO"] + (j - 1) * 2)
+            arrived(wo.at[at_y(-j), V_A:VD, wo_half(c)], M["WO"] + (j - 1) * 2 + 1)
+            send(wo.at[at_y(-j), :, wo_half(c)], wo.at[at_y(-j), :, wo_half(c)], M["WP"] + j, partner)
 
     for j in range(NX):
         ml[j] = jnp.concatenate([jnp.full((2, ROWS), -jnp.inf, F32), jnp.zeros((6, ROWS), F32)], axis=0)
@@ -289,10 +309,12 @@
                 old = ml[j, h : h + 1, :]
                 new = jnp.maximum(old, jnp.max(scores, axis=0, keepdims=True))
                 factor = jnp.exp2((old - new) * scale)
-                raised = jnp.exp2((scores - new) * scale)
+                raised = jnp.exp2((scores - new) * scale).astype(BF16)
                 ml[j, h : h + 1, :] = new
-                ml[j, 2 + h : 3 + h, :] = ml[j, 2 + h : 3 + h, :] * factor + jnp.sum(raised, axis=0, keepdims=True)
-                acc[j, vlo:vhi, :] = acc[j, vlo:vhi, :] * factor + dot(vx[vlo:vhi, :], raised.astype(BF16), ((1,), (0,)))
+                with_ones = jnp.concatenate([vx[vlo:vhi, :], jnp.ones((16, 2 * ROWS), BF16)], axis=0)
+                product = dot(with_ones, raised, ((1,), (0,)))
+                ml[j, 2 + h : 3 + h, :] = ml[j, 2 + h : 3 + h, :] * factor + product[vhi - vlo : vhi - vlo + 1]
+                acc[j, vlo:vhi, :] = acc[j, vlo:vhi, :] * factor + product[0 : vhi - vlo]
 
     def quarter_out(u):
         d = (u + 1) // 2
@@ -325,7 +347,9 @@
 
         on_step(i, 1, lambda: (quarter_out(5), quarter_out(6), quarter_out(7), send_wo(), slots_round(1)))
         on_step(i, 2, lambda: start_rows())
+        on_step(i, 3, lambda: rows_round(1, 0))
         on_step(i, 4, lambda: slots_round(2))
+        on_step(i, 6, lambda: rows_round(1, 1, 3))
 
         @pl.when(i < 7)
         def _():
@@ -345,7 +369,8 @@
         send(osend.at[at_x(j)], orecv.at[j - 1], M["O"] + j, dev_x(j))
         send(ml.at[at_x(j)], srecv.at[j - 1], M["OS"] + j, dev_x(j))
 
-    rows_round(1)
+    rows_round(1, 2)
+    rows_round(2, 0)
     slots_round(3)
     relay(0)
     for j in range(1, NX):
@@ -359,22 +384,30 @@
         shares = [total * jnp.exp2((m - top) * scale) for m, total in zip(tops, sums)]
         total = shares[0] + shares[1] + shares[2] + shares[3]
         mixed = sum(part.astype(F32) * (share / total) for part, share in zip(parts, shares))
-        att[t, vlo:vhi, :] = mixed.astype(BF16)
+        attended[vlo:vhi, :] = mixed
+    mine = attended[...].T.astype(BF16)
+    for q in range(NY):
+        attsend[q] = mine[q * QUART : (q + 1) * QUART]
     for j in (2, 1, 3):
-        send(att.at[t], att.at[t], M["AT"] + j, dev_y(j))
-
+        send(attsend.at[at_y(j)], att.at[t], M["AT"] + j, dev_y(j))
+
+    wo_across()
+    rows_round(2, 1)
     relay(1)
+    rows_round(2, 3)
     relay(2)
 
     for o in local[12:]:
         o.wait()
     for j in range(1, NY):
-        for half, rows in enumerate((slice(0, V_A), slice(V_A, VD))):
-            arrived(wo.at[at_y(-j), rows, :], M["WO"] + (j - 1) * 2 + half)
+        arrived(resq.at[:, pl.ds(pl.multiple_of(at_y(-j) * DW, DW), DW)], M["RS"] + j)
+        arrived(gfull.at[0, :, pl.ds(pl.multiple_of(at_y(-j) * DW, DW), DW)], M["GN"] + j)
+        arrived(gfull.at[1, :, pl.ds(pl.multiple_of(at_y(-j) * DW, DW), DW)], M["GN"] + 4 + j)
+        arrived(wo.at[at_y(-j), :, wo_half(1 - c)], M["WP"] + j)
     for j in range(1, NY):
         arrived(att.at[at_y(-j)], M["AT"] + j)
 
-    def norm(stat, got, first, gain_ref, bias_ref, between):
+    def norm(stat, got, first, gain_ref, bias_ref):
         h = hres[...]
         center = jnp.mean(h, axis=1, keepdims=True)
         apart = jnp.sum((h - center) * (h - center), axis=1, keepdims=True)
@@ -383,7 +416,6 @@
         stat[...] = both.T[0:8]
         for j in (2, 1, 3):
             send(stat, got.at[j - 1], first + j, dev_y(j))
-        between()
         for j in range(1, NY):
             arrived(got.at[j - 1], first + j)
         centers = [stat[0:1, :]] + [got[j, 0:1, :] for j in range(3)]
@@ -394,21 +426,26 @@
         cols = jnp.concatenate([middle, root, jnp.zeros((126, ROWS), F32)], axis=0).T
         return ((h - cols[:, 0:1]) * cols[:, 1:2] * gain_ref[...] + bias_ref[...]).astype(BF16)
 
-    mixed = dot(att[...].reshape(NY * VD, ROWS), wo[...].reshape(NY * VD, DW), ((0,), (0,)))
-    hres[...] = DEEP_ALPHA * res_ref[...].astype(F32) + mixed
-    normed = norm(st1, sr1, M["S1"], g1_ref, b1_ref, lambda: (slots_round(4), relay(3)))
-    xbuf[:, my_cols] = normed
-    hres[...] = DEEP_ALPHA * normed.astype(F32)
+    h = DEEP_ALPHA * resq[...].astype(F32) + dot(attsend[t], wo[t], ((1,), (0,)))
+    for j in range(1, NY):
+        h = h + dot(att[at_y(j)], wo[at_y(j)], ((1,), (0,)))
+    center = jnp.mean(h, axis=1, keepdims=True)
+    spread = jnp.mean((h - center) * (h - center), axis=1, keepdims=True)
+    my_rows = pl.ds(pl.multiple_of(t * QUART, QUART), QUART)
+    xbuf[my_rows, :] = ((h - center) * lax.rsqrt(spread + EPS_LAYER) * gfull[0] + gfull[1]).astype(BF16)
 
     def x_half(off, half):
-        return xbuf.at[pl.ds(half * HALF, HALF), pl.ds(pl.multiple_of(at_y(off) * DW, DW), DW)]
+        return xbuf.at[pl.ds(pl.multiple_of(at_y(off) * QUART, QUART), QUART), pl.ds(half * (D // 2), D // 2)]
 
     def send_x(off, half, i, way):
         send(x_half(off, half), x_half(off, half), M["G"] + i, dev_y(way))
 
     for i, half, way in ((0, 0, 1), (2, 1, -1), (1, 1, 1), (3, 0, -1)):
         send_x(0, half, i, way)
-    rows_round(2)
+    slots_round(4)
+    rows_round(2, 2)
+    relay(3)
+    rows_round(3, 0)
     relay(4)
     across(0)
     across(1)
@@ -416,24 +453,32 @@
     send_x(-1, 0, 4, 1)
     arrived(x_half(1, 1), M["G"] + 2)
     send_x(1, 1, 5, -1)
-    rows_round(3)
+    rows_round(3, 1)
     relay(5)
     across(2)
+    rows_round(3, 3)
     relay(6)
     across(3)
+    rows_round(3, 2)
     relay(7)
     for i, off, half in ((1, -1, 1), (3, 1, 0), (4, 2, 0), (5, 2, 1)):
         arrived(x_half(off, half), M["G"] + i)
 
+    hres[...] = DEEP_ALPHA * xbuf[:, my_cols].astype(F32)
+
     def gate_up(u):
         zu = zz(u)
         features = xbuf[:, pl.ds(pl.multiple_of(zu * 256, 256), 256)]
-        for n in range(WB // 256):
+        for n in range(GU // 256):
             cols = slice(n * 256, (n + 1) * 256)
             part = dot(features, wbuf[zu, :, :, :, cols].reshape(256, 256), ((1,), (0,)))
             gbuf[:, cols] = part if isinstance(u, int) else gbuf[:, cols] + part
 
+    def partner_rows(u):
+        arrived(wbuf.at[zz(u), :, 1 - c, :, A_COLS], M["PA"] + u)
+
     partner_block(0)
+    partner_rows(0)
     gate_up(0)
 
     def block(u, carry):
@@ -441,15 +486,14 @@
         def _():
             across(u + 3)
 
+        on_step(u, 5, lambda: rows_round(4, 0, 1, 3, 2))
+
         partner_block(u)
+        partner_rows(u)
         gate_up(u)
         return carry
 
     lax.fori_loop(1, NZ, block, 0)
-    rows_round(4)
-    for u in range(NZ):
-        arrived(wbuf.at[zz(u), :, 1 - c, :, A_COLS], M["PA"] + u)
-    gbuf[:, WB:GU] = dot(xbuf[...], wbuf[:, :, :, :, WB:GU].reshape(D, 256), ((1,), (0,)))
     gate = gbuf[:, 0:FH]
     hid[...] = (gate / (1.0 + jnp.exp(-gate)) * gbuf[:, FH:GU]).astype(BF16)
 
@@ -478,7 +522,7 @@
     for i, k, rows in ((2, 0, second), (3, 1, first), (4, 0, first), (5, 1, second)):
         arrived(frecv.at[k, rows], M["F"] + i)
     hres[...] += frecv[0].astype(F32) + frecv[1].astype(F32)
-    out_ref[...] = norm(st2, sr2, M["S2"], g2_ref, b2_ref, lambda: None)
+    out_ref[...] = norm(st2, sr2, M["S2"], g2_ref, b2_ref)
 
     for j in range(1, NX):
         sent(qbuf.at[0, 0:96, :], M["Q"] + (j - 1) * 2)
@@ -486,14 +530,19 @@
         sent(a_slot(0, 0), M["A1"] + j)
         sent(osend.at[0], M["O"] + j)
         sent(ml.at[0], M["OS"] + j)
-        sent(wo.at[0, 0:V_A, :], M["WO"] + (j - 1) * 2)
-        sent(wo.at[0, V_A:VD, :], M["WO"] + (j - 1) * 2 + 1)
+        sent(wo.at[0, 0:V_A, wo_half(0)], M["WO"] + (j - 1) * 2)
+        sent(wo.at[0, V_A:VD, wo_half(0)], M["WO"] + (j - 1) * 2 + 1)
+        sent(wo.at[0, :, wo_half(0)], M["WP"] + j)
+        sent(resq.at[:, my_cols], M["RS"] + j)
+        sent(g1_ref, M["GN"] + j)
+        sent(b1_ref, M["GN"] + 4 + j)
         sent(att.at[0], M["AT"] + j)
-        sent(st1, M["S1"] + j)
         sent(st2, M["S2"] + j)
     for d in range(1, 5):
         for way in "MP":
-            sent(a_row(0) if d < 4 else a_row(0).at[0:2], M["A" + way] + d)
+            for r in range(4):
+                if d < 4 or (r >= 2) == (way == "M"):
+                    sent(a_slot(0, 0), M["A" + way] + 4 * d + r)
             if d < 4 or way == "M":
                 sent(b_slot(0, 0), M["B" + way] + d)
     for u in range(NZ):
@@ -538,7 +587,7 @@
         in_specs=[pl.BlockSpec(memory_space=pl.ANY)] * len(large) + [vmem] * len(small),
         out_specs=vmem,
         scratch_shapes=[
-            *[pltpu.VMEM(v.shape, v.dtype) for v in large[:10]],
+            *[pltpu.VMEM(v.shape, v.dtype) for v in large[1:10]],
             pltpu.VMEM((NZ, 2, NY, 80, LAT), BF16),
             pltpu.VMEM((NX, KX, ROWS), BF16),
             pltpu.VMEM((NZ, NX, 2, SLOT, WT), BF16),
@@ -551,10 +600,12 @@
             pltpu.VMEM((NX, VD, ROWS), BF16),
             pltpu.VMEM((3, VD, ROWS), BF16),
             pltpu.VMEM((3, 8, ROWS), F32),
-            pltpu.VMEM((NY, VD, ROWS), BF16),
-            pltpu.VMEM((NY, VD, DW), BF16),
-            pltpu.VMEM((8, ROWS), F32),
-            pltpu.VMEM((3, 8, ROWS), F32),
+            pltpu.VMEM((VD, ROWS), F32),
+            pltpu.VMEM((NY, QUART, VD), BF16),
+            pltpu.VMEM((NY, QUART, VD), BF16),
+            pltpu.VMEM((NY, VD, D), BF16),
+            pltpu.VMEM((QUART, D), BF16),
+            pltpu.VMEM((2, 1, D), F32),
             pltpu.VMEM((8, ROWS), F32),
             pltpu.VMEM((3, 8, ROWS), F32),
             pltpu.VMEM((ROWS, D), BF16),
@@ -567,7 +618,7 @@
             pltpu.VMEM((ROWS, DW), F32),
             pltpu.SemaphoreType.DMA((MESSAGES,)),
             pltpu.SemaphoreType.DMA((MESSAGES,)),
-            pltpu.SemaphoreType.DMA((len(large),)),
+            pltpu.SemaphoreType.DMA((len(large) + 2,)),
         ],
         compiler_params=pltpu.CompilerParams(
             collective_id=0, has_side_effects=True, vmem_limit_bytes=60 * 1024 * 1024

time: 99.6 us -> 95.2 us (0.956)
  Pallas kernels: 95.8 us -> 91.6 us
    pallas_call x1, Pallas kernels: 95.8 us -> 91.6 us  [body(): pl.pallas_call(layer_kernel, out_shape=jax.ShapeDtypeStruct((ROWS, DW), B...]
where the time goes in v4:
time: 95.2 us; the launch traced here: 94.1 us
  Pallas kernels  91.6 us (96%)
  local copies, waits for them, and re-layouts  1.67 us (2%)
    pallas_call x1, Pallas kernels, body(): pl.pallas_call(layer_kernel, out_shape=jax.ShapeDtypeStruct((ROWS, DW), B...  91.6 us

profile of v4, /device:TPU:1, one launch (start us, length us, event | category | flops | bytes accessed | tf_op | source)
XLA Modules:
  0.0 94.1 jit_solution(5036901271862135917)
XLA Ops:
  0.0 0.7 multiply_sine_fusion
  0.8 91.6 %shard_map.199 = bf16[256,512]{1,0:T(8,128)(2,1)} custom-call(bf16[256,512]{1,0:T(8,128)(2,1)} %res_hbm.1, bf16[256,512]{1,0:T(8,128)(2,1)} %ql_hbm.1, bf16[256,256]{1,0:T(8,128)(2,1)} %sl_hbm.1, bf16[32,256]{1,0:T(8,128)(2,1)} %bitcast.17, bf16[96,512]{1,0:T(8,128)(2,1)} %bitcast.13, bf16[64,256]{1,0:T(8,128)(2,1)} %bitcast.15, bf16[64,256]{1,0:T(8,128)(2,1)} %bitcast.16, ...), custom_call_target="tpu_custom_call" | custom-call | tf_op jit(solution)/shard_map/pallas_call | solution.py:584
  92.4 1.7 %copy.23 = bf16[256,512]{1,0:T(8,128)(2,1)} copy(bf16[256,512]{1,0:T(8,128)(2,1)} %shard_map.199) | data formatting | bytes 524288
  (2 shorter events, 0.0 us)

commit v5 on v4

--- a/solution.py
+++ b/solution.py
@@ -27,7 +27,7 @@
 FH = 1408
 GU = 2 * FH
 WT = 3 * FH
-WB = GU - 512
+WB = GU - 640
 B_COLS, A_COLS = slice(0, WB), slice(WB, WT)
 SLOT = 32
 VD = V_A + V_B
@@ -47,8 +47,8 @@
 
 
 M, MESSAGES = numbered(
-    Q=6, KZ=8, KY=24, KT=8, O=4, OS=4, WO=6, WP=4, RS=4, GN=8, AT=4, G=6, F=6, S2=4,
-    A1=4, AM=20, AP=20, BM=5, BP=4, XP=8, XM=8, RL=8, PB=32, PA=8,
+    Q=6, KM=5, KP=4, KY=24, KT=8, O=4, OS=4, WO=6, WP=4, RS=4, GN=8, AT=4, G=6, F=6, S2=4,
+    A1=4, AM=20, AP=20, BM=5, BP=4, XP=8, XM=8, RL=9, PB=32, PA=8,
 )
 
 
@@ -69,7 +69,7 @@
 
 def layer_kernel(
     res_hbm, ql_hbm, sl_hbm, rk_hbm, wqn_hbm, kn_hbm, vn_hbm, wqw_hbm, kw_hbm, vw_hbm, on_ref, ow_ref,
-    gate_ref, up_ref, down_ref, qg_ref, lg_ref, g1_ref, b1_ref, g2_ref, b2_ref, cr_ref, sr_ref, cc_ref, sc_ref,
+    gate_ref, up_ref, down_ref, qg_ref, lg_ref, g1_ref, b1_ref, g2_ref, b2_ref,
     out_ref,
     ql_ref, sl_ref, rk_ref, wqn_ref, kn_ref, vn_ref, wqw_ref, kw_ref, vw_ref,
     kvbuf, qbuf, wbuf, wk, wv, kx, vx, ml, acc, osend, orecv, srecv, attended, attsend, att, wo, resq, gfull, st2, sr2,
@@ -124,7 +124,7 @@
     a_row = lambda zi: wbuf.at[zi, :, c, :, A_COLS]
 
     barrier = pltpu.get_barrier_semaphore()
-    friends = [*[dev_z(off) for off in range(1, NZ)], dev_x(1), dev_x(2), dev_x(3), partner, dev_y(1), dev_y(2), dev_y(3)]
+    friends = [dev_z(1), dev_z(-1), dev_x(1), dev_x(2), dev_x(3), partner, dev_y(1), dev_y(2), dev_y(3)]
     for f in friends:
         pl.semaphore_signal(barrier, inc=1, device_id=f, device_id_type=MESH)
 
@@ -143,7 +143,14 @@
     for o in local[:9]:
         o.wait()
 
-    tab = (cr_ref[...], sr_ref[...], cc_ref[...], sc_ref[...])
+    quarter = lax.broadcasted_iota(jnp.int32, (8, ROWS), 0)
+    at = lax.broadcasted_iota(jnp.int32, (8, ROWS), 1)
+    freq = jnp.ones((8, ROWS), F32)
+    for i in range(1, 8):
+        freq = jnp.where(quarter == i, THETA ** (-2.0 * i / 16), freq)
+    row_angle = (s * (ROWS // GRID_W) + at // GRID_W).astype(F32) * freq
+    col_angle = (at % GRID_W).astype(F32) * freq
+    tab = (jnp.cos(row_angle), jnp.sin(row_angle), jnp.cos(col_angle), jnp.sin(col_angle))
     latent = root_scale(sl_ref[...], lg_ref[...]).astype(BF16)
     turned = turn(rk_ref[...].astype(F32), tab)
     for q in range(NY):
@@ -164,8 +171,8 @@
 
     pl.semaphore_wait(barrier, len(friends))
 
-    for off in (1, 7, 2, 6, 3, 5, 4):
-        send(kvbuf.at[z, c, t], kvbuf.at[z, c, t], M["KZ"] + off, dev_z(off))
+    send(kvbuf.at[z, c, t], kvbuf.at[z, c, t], M["KM"] + 1, dev_z(-1))
+    send(kvbuf.at[z, c, t], kvbuf.at[z, c, t], M["KP"] + 1, dev_z(1))
     send(kvbuf.at[z, c], kvbuf.at[z, c], M["KT"], partner)
     for j in (2, 1, 3):
         for half, rows in enumerate((slice(0, 96), slice(224, 384))):
@@ -199,11 +206,12 @@
         send(b_slot(z, x), b_slot(z, x), M["BP"] + 1, dev_z(1))
         to_partner(0, z, 0)
 
-    def start_rows():
-        for r in (1, 3, 2):
+    def start_rows(*rs):
+        for r in rs:
             arrived(a_slot(z, at_x(-r)), M["A1"] + r)
             send_rows(z, 1, r)
-        row_to_partner(0, z)
+        if 2 in rs:
+            row_to_partner(0, z)
 
     def rows_round(d, *rs):
         below, above = at_z(-d), at_z(d)
@@ -239,19 +247,26 @@
 
     plus = (0, 1, 3, 5)
 
+    def part(u, zi, xi, way):
+        slot = b_slot(zi, xi)
+        return slot.at[pl.ds(way * SLOT // 2, SLOT // 2), :] if u == 7 else slot
+
     def relay(u):
         zu = zz(u)
         arrived(b_slot(zu, at_x(-1)), M["XP"] + u)
-        if u in plus:
-            send(b_slot(zu, at_x(-1)), b_slot(zu, at_x(-1)), M["RL"] + u, dev_x(1))
+        if u in plus or u == 7:
+            send(part(u, zu, at_x(-1), 0), part(u, zu, at_x(-1), 0), M["RL"] + u, dev_x(1))
         to_partner(u, zu, 1)
         arrived(b_slot(zu, at_x(1)), M["XM"] + u)
         if u not in plus:
-            send(b_slot(zu, at_x(1)), b_slot(zu, at_x(1)), M["RL"] + u, dev_x(-1))
+            i = u + 1 if u == 7 else u
+            send(part(u, zu, at_x(1), 1), part(u, zu, at_x(1), 1), M["RL"] + i, dev_x(-1))
         to_partner(u, zu, 2)
 
     def across(u):
-        arrived(b_slot(zz(u), at_x(2)), M["RL"] + u)
+        last = isinstance(u, int) and u == 7
+        for way in range(2 if last else 1):
+            arrived(part(7 if last else 0, zz(u), at_x(2), way), M["RL"] + u + way)
         to_partner(u, zz(u), 3)
 
     def partner_block(u):
@@ -317,9 +332,12 @@
                 acc[j, vlo:vhi, :] = acc[j, vlo:vhi, :] * factor + product[0 : vhi - vlo]
 
     def quarter_out(u):
-        d = (u + 1) // 2
+        d, upwards = (u + 1) // 2, u % 2 and u != 7
         slot = kvbuf.at[zz(u), c, t]
-        arrived(slot, M["KZ"] + (d if u % 2 else NZ - d))
+        first = M["KP"] if upwards else M["KM"]
+        arrived(slot, first + d)
+        if d < (3 if upwards else 4):
+            send(slot, slot, first + d + 1, dev_z(1 if upwards else -1))
         for j in (2, 1, 3):
             send(slot, slot, M["KY"] + 3 * u + j - 1, dev_y(j))
 
@@ -337,19 +355,18 @@
     def unit(i, carry):
         @pl.when(i == 0)
         def _():
-            quarter_out(1)
-            quarter_out(2)
+            for u in range(1, 5):
+                quarter_out(u)
             for j in range(1, NX):
                 for half, rows in enumerate((slice(0, 96), slice(224, 384))):
                     arrived(qbuf.at[at_x(-j), rows, :], M["Q"] + (j - 1) * 2 + half)
-            quarter_out(3)
-            quarter_out(4)
-
-        on_step(i, 1, lambda: (quarter_out(5), quarter_out(6), quarter_out(7), send_wo(), slots_round(1)))
-        on_step(i, 2, lambda: start_rows())
+
+        on_step(i, 1, lambda: (quarter_out(5), quarter_out(6), slots_round(1)))
+        on_step(i, 2, lambda: (quarter_out(7), send_wo(), start_rows(1)))
         on_step(i, 3, lambda: rows_round(1, 0))
         on_step(i, 4, lambda: slots_round(2))
-        on_step(i, 6, lambda: rows_round(1, 1, 3))
+        on_step(i, 5, lambda: start_rows(3, 2))
+        on_step(i, 6, lambda: rows_round(1, 1))
 
         @pl.when(i < 7)
         def _():
@@ -369,10 +386,10 @@
         send(osend.at[at_x(j)], orecv.at[j - 1], M["O"] + j, dev_x(j))
         send(ml.at[at_x(j)], srecv.at[j - 1], M["OS"] + j, dev_x(j))
 
-    rows_round(1, 2)
-    rows_round(2, 0)
+    relay(0)
     slots_round(3)
-    relay(0)
+    relay(1)
+    rows_round(1, 3)
     for j in range(1, NX):
         arrived(orecv.at[j - 1], M["O"] + j)
         arrived(srecv.at[j - 1], M["OS"] + j)
@@ -392,10 +409,12 @@
         send(attsend.at[at_y(j)], att.at[t], M["AT"] + j, dev_y(j))
 
     wo_across()
+    relay(2)
+    relay(3)
+    rows_round(1, 2)
+    rows_round(2, 0)
+    relay(4)
     rows_round(2, 1)
-    relay(1)
-    rows_round(2, 3)
-    relay(2)
 
     for o in local[12:]:
         o.wait()
@@ -443,24 +462,21 @@
     for i, half, way in ((0, 0, 1), (2, 1, -1), (1, 1, 1), (3, 0, -1)):
         send_x(0, half, i, way)
     slots_round(4)
-    rows_round(2, 2)
-    relay(3)
-    rows_round(3, 0)
-    relay(4)
-    across(0)
-    across(1)
+    relay(5)
     arrived(x_half(-1, 0), M["G"])
     send_x(-1, 0, 4, 1)
     arrived(x_half(1, 1), M["G"] + 2)
     send_x(1, 1, 5, -1)
+    rows_round(2, 3, 2)
+    relay(6)
+    across(0)
+    across(1)
+    rows_round(3, 0)
+    across(2)
     rows_round(3, 1)
-    relay(5)
-    across(2)
-    rows_round(3, 3)
-    relay(6)
     across(3)
-    rows_round(3, 2)
     relay(7)
+    rows_round(3, 3, 2)
     for i, off, half in ((1, -1, 1), (3, 1, 0), (4, 2, 0), (5, 2, 1)):
         arrived(x_half(off, half), M["G"] + i)
 
@@ -482,10 +498,11 @@
     gate_up(0)
 
     def block(u, carry):
-        @pl.when(u <= 4)
+        @pl.when(u <= 3)
         def _():
             across(u + 3)
 
+        on_step(u, 4, lambda: across(7))
         on_step(u, 5, lambda: rows_round(4, 0, 1, 3, 2))
 
         partner_block(u)
@@ -518,12 +535,6 @@
     arrived(fthru.at[1], M["F"] + 1)
     fsend[2, second] = (fkeep[1] + fthru[1].astype(F32)).astype(BF16)
     send(fsend.at[2, second], frecv.at[1, second], M["F"] + 5, dev_y(-1))
-    hres[...] += feed(0)
-    for i, k, rows in ((2, 0, second), (3, 1, first), (4, 0, first), (5, 1, second)):
-        arrived(frecv.at[k, rows], M["F"] + i)
-    hres[...] += frecv[0].astype(F32) + frecv[1].astype(F32)
-    out_ref[...] = norm(st2, sr2, M["S2"], g2_ref, b2_ref)
-
     for j in range(1, NX):
         sent(qbuf.at[0, 0:96, :], M["Q"] + (j - 1) * 2)
         sent(qbuf.at[0, 224:384, :], M["Q"] + (j - 1) * 2 + 1)
@@ -537,7 +548,6 @@
         sent(g1_ref, M["GN"] + j)
         sent(b1_ref, M["GN"] + 4 + j)
         sent(att.at[0], M["AT"] + j)
-        sent(st2, M["S2"] + j)
     for d in range(1, 5):
         for way in "MP":
             for r in range(4):
@@ -548,16 +558,27 @@
     for u in range(NZ):
         sent(kvbuf.at[0, 0], M["KT"] + u)
         if u > 0:
-            sent(kvbuf.at[0, 0, 0], M["KZ"] + u)
+            sent(kvbuf.at[0, 0, 0], M["KM"] + u if u < 5 else M["KP"] + u - 4)
             for j in range(1, NY):
                 sent(kvbuf.at[0, 0, 0], M["KY"] + 3 * u + j - 1)
         sent(a_row(0), M["PA"] + u)
         for way in range(4):
             sent(b_slot(0, 0), M["PB"] + 4 * u + way)
-        for name in ("XP", "XM", "RL"):
+        for name in ("XP", "XM"):
             sent(b_slot(0, 0), M[name] + u)
+        sent(part(u, 0, 0, 0), M["RL"] + u)
+    sent(part(7, 0, 0, 1), M["RL"] + 8)
     for i in range(6):
         sent(x_half(0, 0), M["G"] + i)
+    hres[...] += feed(0)
+    for i, k, rows in ((2, 0, second), (3, 1, first), (4, 0, first), (5, 1, second)):
+        arrived(frecv.at[k, rows], M["F"] + i)
+    hres[...] += frecv[0].astype(F32) + frecv[1].astype(F32)
+    out_ref[...] = norm(st2, sr2, M["S2"], g2_ref, b2_ref)
+
+    for j in range(1, NX):
+        sent(st2, M["S2"] + j)
+    for i in range(6):
         sent(fsend.at[0, 0:HALF], M["F"] + i)
 
 
@@ -566,11 +587,6 @@
     value_narrow, query_wide, key_wide, value_wide, output_narrow, output_wide, first_gain, first_bias,
     gate_weight, up_weight, down_weight, second_gain, second_bias,
 ):
-    positions = lax.axis_index("sp") * ROWS + jnp.arange(ROWS, dtype=jnp.int32)
-    quarter = ROPE // 4
-    freqs = THETA ** (-(2.0 * jnp.arange(quarter, dtype=F32)) / (2 * quarter))
-    row_angle = freqs[:, None] * (positions // GRID_W).astype(F32)[None, :]
-    col_angle = freqs[:, None] * (positions % GRID_W).astype(F32)[None, :]
     row = lambda v: v.reshape(1, -1)
     large = (
         residual, query_latent, shared_latent, rotary_key.T, query_narrow.T, key_narrow.T, value_narrow.T,
@@ -578,7 +594,6 @@
     )
     small = (
         row(query_gain), row(latent_gain), row(first_gain), row(first_bias), row(second_gain), row(second_bias),
-        jnp.cos(row_angle), jnp.sin(row_angle), jnp.cos(col_angle), jnp.sin(col_angle),
     )
     vmem = pl.BlockSpec(memory_space=pltpu.VMEM)
     return pl.pallas_call(

time: 95.2 us -> 93.9 us (0.986)
  no operation moved by 1% of the time
where the time goes in v5:
time: 93.9 us; the launch traced here: 93.2 us
  Pallas kernels  91.5 us (97%)
  local copies, waits for them, and re-layouts  1.67 us (2%)
    pallas_call x1, Pallas kernels, body(): pl.pallas_call(layer_kernel, out_shape=jax.ShapeDtypeStruct((ROWS, DW), B...  91.5 us

profile of v5, /device:TPU:1, one launch (start us, length us, event | category | flops | bytes accessed | tf_op | source)
XLA Modules:
  0.0 93.2 jit_solution(13597556497755354320)
XLA Ops:
  0.0 91.5 %shard_map.199 = bf16[256,512]{1,0:T(8,128)(2,1)} custom-call(bf16[256,512]{1,0:T(8,128)(2,1)} %res_hbm.1, bf16[256,512]{1,0:T(8,128)(2,1)} %ql_hbm.1, bf16[256,256]{1,0:T(8,128)(2,1)} %sl_hbm.1, bf16[32,256]{1,0:T(8,128)(2,1)} %bitcast.17, bf16[96,512]{1,0:T(8,128)(2,1)} %bitcast.13, bf16[64,256]{1,0:T(8,128)(2,1)} %bitcast.15, bf16[64,256]{1,0:T(8,128)(2,1)} %bitcast.16, ...), custom_call_target="tpu_custom_call" | custom-call | tf_op jit(solution)/shard_map/pallas_call | solution.py:599
  91.5 1.7 %copy.23 = bf16[256,512]{1,0:T(8,128)(2,1)} copy(bf16[256,512]{1,0:T(8,128)(2,1)} %shard_map.199) | data formatting | bytes 524288

commit v6 on v5

--- a/solution.py
+++ b/solution.py
@@ -27,7 +27,7 @@
 FH = 1408
 GU = 2 * FH
 WT = 3 * FH
-WB = GU - 640
+WB = GU - 512
 B_COLS, A_COLS = slice(0, WB), slice(WB, WT)
 SLOT = 32
 VD = V_A + V_B

time: 93.9 us -> 94.5 us (level)
  Pallas kernels: 91.5 us -> 92.7 us
    pallas_call x1, Pallas kernels: 91.5 us -> 92.7 us  [body(): pl.pallas_call(layer_kernel, out_shape=jax.ShapeDtypeStruct((ROWS, DW), B...]
where the time goes in v6:
time: 94.5 us; the launch traced here: 94.4 us
  Pallas kernels  92.7 us (98%)
  local copies, waits for them, and re-layouts  1.67 us (2%)
    pallas_call x1, Pallas kernels, body(): pl.pallas_call(layer_kernel, out_shape=jax.ShapeDtypeStruct((ROWS, DW), B...  92.7 us

profile of v6, /device:TPU:1, one launch (start us, length us, event | category | flops | bytes accessed | tf_op | source)
XLA Modules:
  0.0 94.4 jit_solution(6677019135341065870)
XLA Ops:
  0.0 92.7 %shard_map.199 = bf16[256,512]{1,0:T(8,128)(2,1)} custom-call(bf16[256,512]{1,0:T(8,128)(2,1)} %res_hbm.1, bf16[256,512]{1,0:T(8,128)(2,1)} %ql_hbm.1, bf16[256,256]{1,0:T(8,128)(2,1)} %sl_hbm.1, bf16[32,256]{1,0:T(8,128)(2,1)} %bitcast.17, bf16[96,512]{1,0:T(8,128)(2,1)} %bitcast.13, bf16[64,256]{1,0:T(8,128)(2,1)} %bitcast.15, bf16[64,256]{1,0:T(8,128)(2,1)} %bitcast.16, ...), custom_call_target="tpu_custom_call" | custom-call | tf_op jit(solution)/shard_map/pallas_call | solution.py:599
  92.7 1.7 %copy.23 = bf16[256,512]{1,0:T(8,128)(2,1)} copy(bf16[256,512]{1,0:T(8,128)(2,1)} %shard_map.199) | data formatting | bytes 524288
